TPU v7x, 128 devices: a whole 4x4x4 slice. The times are simulated.
128 devices in a mesh: sp: 16 (over z, x), fs: 4 (over y), tp: 2 (over core).
Axes of the slice: x: 4, y: 4, z: 4, core: 2. Of those that a mesh axis runs over, the one named last changes fastest.
Arguments:
- stream: bfloat16 [4, 16384, 2048], P('fs', 'sp', 'tp'), parts along dimension 0, may hold values from -6 to 6
- w_pool_in: bfloat16 [2048, 1024], P(None, 'tp'), may hold values from -0.125 to 0.125
- w_query: bfloat16 [2048, 1024], P(None, 'tp'), may hold values from -0.125 to 0.125
- w_forget: bfloat16 [2048, 1024], P(None, 'tp'), may hold values from -0.125 to 0.125
- w_value: bfloat16 [2048, 1024], P(None, 'tp'), may hold values from -0.125 to 0.125
- w_outgate: bfloat16 [2048, 1024], P(None, 'tp'), may hold values from -0.125 to 0.125
- pool_mix: bfloat16 [4, 256, 256], P('tp'), may hold values from -0.375 to 0.375
- pool_scale: float32 [1024], P('tp'), may hold values from 0.1 to 1.9
- lower_bound: float32 [1024], P('tp'), may hold values from 0.9 to 1
- extra_decay: float32 [16384, 8], P('sp', 'tp'), may hold values from -0.7 to 0
- rec_gain: float32 [128], replicated, may hold values from 0.1 to 1.9
- w_out_pool: bfloat16 [1024, 2048], P('tp'), may hold values from -0.125 to 0.125
- w_out_rec: bfloat16 [1024, 2048], P('tp'), may hold values from -0.125 to 0.125
- norm_gain: float32 [2048], P('tp'), may hold values from 0.1 to 1.9
- norm_bias: float32 [2048], P('tp'), may hold values from -3 to 3
Outputs:
- layer_out: bfloat16 [4, 16384, 2048], P('fs', 'sp', 'tp'), parts along dimension 0
There are 4 independent parts, one for each index of `fs`. A program takes and returns all parts, laid end to end along the dimension named above; an argument that names none is the same for every part. Nothing has to cross between parts.
All inputs are finite; a program needn't handle non-finite values.
Results may differ from a plain program's by a relative error of at most 0.0085.
Values may be sent and summed in bfloat16 or wider, within the bound.
A program may use at most 128 MiB of HBM per device.

v0:
```python
import jax
import jax.numpy as jnp
from jax import lax
from jax.sharding import Mesh
from jax.sharding import PartitionSpec as P

D = 2048
DK = 128
WMAX = 16
BLOCK_ROWS = 128
GROUP_CH = 256
SP = ("sp_0", "sp_1")


ALPHA = 2.0**0.25
EPS_RMS = 1e-06
EPS_NORM = 1e-05


def filled_with(x, identity):
    return jax.tree.map(
        lambda a, e: jnp.broadcast_to(jnp.asarray(e, a.dtype), a.shape), x, identity
    )


def gathered_once(x, axis):
    leaves = jax.tree.leaves(x)
    turns = sorted(range(len(leaves)), key=lambda k: -leaves[k].size)
    width = (1, *leaves[turns[0]].shape)[-1]
    lines = [
        jnp.pad(leaves[k].reshape(-1), (0, -leaves[k].size % width)).reshape(-1, width)
        for k in turns
    ]
    both, at, found = (lax.all_gather(jnp.concatenate(lines), axis), 0, {})
    for k, line in zip(turns, lines):
        section = both[:, at : at + len(line)].reshape(len(both), -1)
        found[k] = section[:, : leaves[k].size].reshape(-1, *leaves[k].shape)
        at += len(line)
    numbers = iter(range(len(leaves)))
    return jax.tree.map(lambda _: found[next(numbers)], x)


def entering(x, axes, combine, identity):
    before = start = filled_with(x, identity)
    subtotal = x
    for axis in reversed(axes):
        devices, mine = (lax.axis_size(axis), lax.axis_index(axis))
        pieces = gathered_once(
            jax.tree.map(
                lambda part, kind: part.astype(kind),
                subtotal,
                (jnp.bfloat16, jnp.bfloat16, jnp.bfloat16, jnp.bfloat16),
            ),
            axis,
        )
        inside, subtotal = (start, start)
        for k in range(devices):
            passed = k < mine
            subtotal = combine(
                subtotal, jax.tree.map(lambda part, own: part[k].astype(own.dtype), pieces, x)
            )
            inside = jax.tree.map(lambda new, old: jnp.where(passed, new, old), subtotal, inside)
        before = combine(inside, before)
    return before


def split_up(x, dim, devices):
    before, after = (x.shape[:dim], x.shape[dim + 1 :])
    return jnp.moveaxis(x.reshape(*before, devices, -1, *after), dim, 0)


def summed_on_arrival(x, axis, dim):
    devices = lax.axis_size(axis)
    pieces = lax.all_to_all(split_up(x, dim, devices), axis, 0, 0, tiled=True)
    return jnp.sum(pieces, axis=0)


def total_of_pieces(x, axis):
    pieces = lax.all_gather(x, axis)
    return pieces.sum(axis=0)


def local(
    stream,
    w_pool_in,
    w_query,
    w_forget,
    w_value,
    w_outgate,
    pool_mix,
    pool_scale,
    lower_bound,
    extra_decay,
    rec_gain,
    w_out_pool,
    w_out_rec,
    norm_gain,
    norm_bias,
):
    features = stream[0]
    length = features.shape[0]
    weights = (w_pool_in, w_query, w_forget, w_value, w_outgate)
    column_piece = lax.all_gather(features, "tp", axis=1, tiled=True)
    projected = tuple(
        (jnp.dot(column_piece, weight, preferred_element_type=jnp.float32) for weight in weights)
    )
    pooled, queries, forget_in, value_in, gate_in = [
        projection.astype(jnp.bfloat16) for projection in projected
    ]
    pool_width = pooled.shape[1]
    tail_rows = pooled[length - (WMAX - 1) :]
    channels = lower_bound.shape[0]
    heads_here = channels // DK
    blocks = length // BLOCK_ROWS
    forget = lower_bound + (1.0 - lower_bound) * jax.nn.sigmoid(forget_in.astype(jnp.float32))
    log_keep = (jnp.log(forget).reshape(length, heads_here, DK) + extra_decay[:, :, None]).reshape(
        length, channels
    )
    weight_in = 1.0 - forget
    squashed = jax.nn.silu(queries.astype(jnp.float32))
    row_ids = lax.broadcasted_iota(jnp.int32, (BLOCK_ROWS, BLOCK_ROWS), 0)
    col_ids = lax.broadcasted_iota(jnp.int32, (BLOCK_ROWS, BLOCK_ROWS), 1)
    lower_mask = (row_ids >= col_ids).astype(jnp.float32)
    keep_blocks = log_keep.reshape(blocks, BLOCK_ROWS, channels)
    log_total = jnp.einsum("ts,bsc->btc", lower_mask, keep_blocks)
    log_end = log_total[:, BLOCK_ROWS - 1]
    query_blocks = squashed.reshape(blocks, BLOCK_ROWS, channels)
    input_blocks = weight_in.reshape(blocks, BLOCK_ROWS, channels)
    value_heads = value_in.reshape(blocks, BLOCK_ROWS, heads_here, DK)
    query_up = (query_blocks * jnp.exp(log_total)).reshape(blocks, BLOCK_ROWS, heads_here, DK)
    input_down = (input_blocks * jnp.exp(-log_total)).reshape(blocks, BLOCK_ROWS, heads_here, DK)
    scores = jnp.einsum("bthd,bshd->bhts", query_up, input_down) * lower_mask[None, None]
    inside = jnp.einsum(
        "bhts,bshe->bthe",
        scores.astype(jnp.bfloat16),
        value_heads,
        preferred_element_type=jnp.float32,
    )
    in_weight = (input_blocks * jnp.exp(log_end[:, None] - log_total)).astype(jnp.bfloat16)
    own_terms = jnp.einsum(
        "bshd,bshe->bhde",
        in_weight.reshape(blocks, BLOCK_ROWS, heads_here, DK),
        value_heads,
        preferred_element_type=jnp.float32,
    )

    def block_step(carry, inputs):
        state, offset = carry
        end_blk, term_blk = inputs
        new_state = jnp.exp(end_blk).reshape(heads_here, DK)[:, :, None] * state + term_blk
        return ((new_state, offset + end_blk), (state, offset))

    start_carry = (
        jnp.zeros((heads_here, DK, DK), jnp.float32),
        jnp.zeros((channels,), jnp.float32),
    )
    final_carry, befores = lax.scan(block_step, start_carry, (log_end, own_terms))
    states_before, offsets_before = befores
    carried = jnp.einsum("bthd,bhde->bthe", query_up, states_before)
    local_out = (inside + carried).reshape(length, heads_here, DK)
    query_far = (query_blocks * jnp.exp(offsets_before[:, None] + log_total)).reshape(
        length, heads_here, DK
    )
    local_state = final_carry[0]
    local_keep = jnp.exp(final_carry[1]).reshape(heads_here, DK)
    unit_keep = jnp.ones_like(local_keep)
    empty_state = jnp.zeros_like(local_state)

    def join_all(earlier, later):
        present = later[3] > 0
        return (
            earlier[0] * later[0],
            later[0][:, :, None] * earlier[1] + later[1],
            jnp.where(present, later[2], earlier[2]),
            jnp.maximum(earlier[3], later[3]),
        )

    empty_rows = jnp.zeros(tail_rows.shape, jnp.float32)
    scanned = entering(
        (local_keep, local_state, tail_rows.astype(jnp.float32), jnp.ones((1,), jnp.float32)),
        SP,
        join_all,
        (unit_keep, empty_state, empty_rows, jnp.zeros((1,), jnp.float32)),
    )
    incoming = scanned[1]
    halo_rows = scanned[2].astype(jnp.bfloat16)
    rec_raw = local_out + jnp.einsum("thd,hde->the", query_far, incoming)
    rec_norm = (
        rec_raw
        * lax.rsqrt(jnp.mean(rec_raw * rec_raw, axis=-1, keepdims=True) + EPS_RMS)
        * rec_gain
    )
    gated = rec_norm * jax.nn.silu(gate_in.astype(jnp.float32)).reshape(length, heads_here, DK)
    rec_out = gated.reshape(length, channels).astype(jnp.bfloat16)
    padded = jnp.concatenate([halo_rows, pooled], axis=0).astype(jnp.float32)
    channel_ids = lax.axis_index("tp") * pool_width + lax.iota(jnp.int32, pool_width)
    group_id = channel_ids // GROUP_CH
    window_len = jnp.left_shift(jnp.ones_like(group_id), group_id + 1)
    window_sum = jnp.zeros((length, pool_width), jnp.float32)
    for lag_rows in range(WMAX):
        lagged = padded[WMAX - 1 - lag_rows : WMAX - 1 - lag_rows + length]
        window_sum = window_sum + jnp.where(
            lag_rows < window_len[None, :], lagged, jnp.float32(0.0)
        )
    position = (lax.axis_index(SP) * length + lax.iota(jnp.int32, length) + 1).astype(jnp.float32)
    counts = jnp.minimum(position[:, None], window_len.astype(jnp.float32)[None, :])
    pool_diff = (window_sum / counts - pooled.astype(jnp.float32)).astype(jnp.bfloat16)
    groups_here = pool_mix.shape[0]
    mixed_groups = jnp.einsum(
        "tgc,gcd->tgd",
        pool_diff.reshape(length, groups_here, GROUP_CH),
        pool_mix,
        preferred_element_type=jnp.float32,
    )
    pool_out = (mixed_groups.reshape(length, pool_width) * pool_scale).astype(jnp.bfloat16)
    contract = (((0,), (1,)), ((), ()))
    mixed = summed_on_arrival(
        lax.dot_general(w_out_pool, pool_out, contract, preferred_element_type=jnp.float32)
        + lax.dot_general(w_out_rec, rec_out, contract, preferred_element_type=jnp.float32),
        "tp",
        0,
    ).T
    resid = ALPHA * features.astype(jnp.float32) + mixed
    row_total, squares = (
        total_of_pieces(jnp.sum(resid, axis=1), "tp"),
        total_of_pieces(jnp.sum(resid * resid, axis=1), "tp"),
    )
    row_mean = (row_total / D)[:, None]
    row_var = (squares / D)[:, None] - row_mean * row_mean
    normed = (resid - row_mean) * lax.rsqrt(row_var + EPS_NORM) * norm_gain + norm_bias
    return normed.astype(jnp.bfloat16)[None]


def solution(mesh):
    torus = Mesh(
        mesh.devices.reshape(4, 4, mesh.shape["fs"], mesh.shape["tp"]), ("sp_0", "sp_1", "fs", "tp")
    )
    return jax.shard_map(
        local,
        mesh=torus,
        in_specs=(
            P("fs", SP, "tp"),
            P(None, "tp"),
            P(None, "tp"),
            P(None, "tp"),
            P(None, "tp"),
            P(None, "tp"),
            P("tp", None, None),
            P("tp"),
            P("tp"),
            P(SP, "tp"),
            P(),
            P("tp", None),
            P("tp", None),
            P("tp"),
            P("tp"),
        ),
        out_specs=P("fs", SP, "tp"),
        check_vma=False,
    )
```

profile of v0, /device:TPU:1, one launch (start us, length us, event | category | flops | bytes accessed | tf_op | source)
XLA Modules:
  0.0 219.5 jit_solution(1167471921932692626)
XLA Ops:
  7.7 1.9 copy.110
  15.9 13.1 %all-gather.9.cloned.1.call-done = bf16[1,1024,2048]{2,1,0:T(8,128)(2,1)} async-done(((bf16[1,1024,1024]{2,1,0:T(8,128)(2,1)}), bf16[1,1024,2048]{2,1,0:T(8,128)(2,1)}) %all-gather.9.cloned.1.call-update) | async-done | bytes 4194320 | tf_op jit(solution)/shard_map/all_gather | solution.py:103
  29.0 5.2 %fusion.47 = bf16[1024,512]{1,0:T(8,128)(2,1)S(1)} fusion(bf16[2048,512]{1,0:T(8,128)(2,1)} %param.18, bf16[1,1024,2048]{2,1,0:T(8,128)(2,1)} %all-gather.9.cloned.1.call-done), kind=kOutput, calls=%fused_computation.83 | convolution fusion | flops 2148007936 | bytes 7340032 | tf_op jit(solution)/shard_map/dot_general | solution.py:105
  34.2 1.0 copy-done.6
  35.2 6.2 %fusion.44 = bf16[1024,512]{1,0:T(8,128)(2,1)} fusion(bf16[2048,512]{1,0:T(8,128)(2,1)} %param.21, bf16[1,1024,2048]{2,1,0:T(8,128)(2,1)} %all-gather.9.cloned.1.call-done), kind=kOutput, calls=%fused_computation.82 | convolution fusion | flops 2148007936 | bytes 7340032 | tf_op jit(solution)/shard_map/dot_general | solution.py:105
  41.4 1.3 reshape.465
  42.7 8.2 %broadcast_subtract_fusion = (f32[1024,512]{1,0:T(8,128)}, f32[1024,512]{1,0:T(8,128)}) fusion(bf16[2048,512]{1,0:T(8,128)(2,1)} %param.20, bf16[1,1024,2048]{2,1,0:T(8,128)(2,1)} %all-gather.9.cloned.1.call-done, f32[512]{0:T(512)S(1)} %broadcast_subtract_fusion.1, f32[512]{0:T(512)S(1)} %copy-done.18), kind=kOutput, calls=%fused_computation.92 | convolution fusion | flops 2151677952 | bytes 10489856 | tf_op jit(solution)/shard_map/dot_general | solution.py:105
  51.0 2.9 %copy.78 = f32[8,128,512]{1,2,0:T(8,128)} copy(f32[8,128,512]{2,1,0:T(8,128)} %bitcast.273) | data formatting | bytes 4194304 | tf_op jit(solution)/shard_map/reshape | solution.py:128
  53.9 2.9 %copy.76 = f32[8,128,512]{1,0,2:T(8,128)} copy(f32[8,128,512]{2,1,0:T(8,128)} %bitcast.272) | data formatting | bytes 4194304 | tf_op jit(solution)/shard_map/reshape | solution.py:116
  56.8 2.4 %bitcast_add_fusion.2 = bf16[8,128,512]{1,0,2:T(8,128)(2,1)S(1)} fusion(f32[8,128,512]{1,0,2:T(8,128)} %copy.76, f32[64,8,8,128]{3,2,1,0:T(8,128)} %copy.110), kind=kLoop, calls=%fused_computation.30 | loop fusion | flops 1048576 | bytes 5242880 | tf_op jit(solution)/shard_map/add | solution.py:116
  59.7 1.2 slice_reduce_fusion
  62.0 1.8 fusion.68
  63.8 15.4 %while.17 = (s32[]{:T(128)}, f32[4,128,128]{2,1,0:T(8,128)S(1)}, f32[512]{0:T(512)S(1)}, bf16[8,4,128,128]{3,2,1,0:T(8,128)(2,1)}, f32[8,512]{1,0:T(8,128)S(1)},...) while((s32[]{:T(128)}, f32[4,128,128]{2,1,0:T(8,128)S(1)}, ...), condition=%wide.region_1.2_spmd.clone, body=%wide.region_0.1_spmd.clone.sunk | while | flops 263171 | bytes 1200257 | solution.py:157
  64.5 1.1 bitcast_add_fusion.9
  66.5 1.1 bitcast_add_fusion.9
  68.4 1.1 bitcast_add_fusion.9
  70.3 1.1 bitcast_add_fusion.9
  72.2 1.1 bitcast_add_fusion.9
  74.2 1.1 bitcast_add_fusion.9
  76.1 1.1 bitcast_add_fusion.9
  78.0 1.1 bitcast_add_fusion.9
  79.2 11.5 %all-gather.5 = bf16[4,577,128]{2,1,0:T(8,128)(2,1)S(1)} all-gather(bf16[1,577,128]{2,1,0:T(8,128)(2,1)S(1)} %maximum_bitcast_fusion), channel_id=3, replica_groups=mesh['sp_0'=4,'sp_1'=4,'fs'=4,'tp'=2] {'sp_1'}, dimensions={0}, use_global_device_ids=true | all-gather | bytes 738560 | tf_op jit(solution)/shard_map/all_gather | solution.py:34
  97.9 11.0 %all-gather.6 = bf16[4,577,128]{2,1,0:T(8,128)(2,1)S(1)} all-gather(bf16[1,577,128]{2,1,0:T(8,128)(2,1)S(1)} %maximum_bitcast_fusion.1), channel_id=4, replica_groups=mesh['sp_0'=4,'sp_1'=4,'fs'=4,'tp'=2] {'sp_0'}, dimensions={0}, use_global_device_ids=true | all-gather | bytes 738560 | tf_op jit(solution)/shard_map/all_gather | solution.py:34
  111.4 0.9 slice_convert_fusion.3
  112.4 5.5 %convert_multiply_fusion.1 = f32[1024,512]{1,0:T(8,128)} fusion(bf16[2048,512]{1,0:T(8,128)(2,1)} %param.19, bf16[1,1024,2048]{2,1,0:T(8,128)(2,1)S(1)} %copy-done.38), kind=kOutput, calls=%fused_computation.21 | convolution fusion | flops 2150629376 | bytes 8388608 | tf_op jit(solution)/shard_map/dot_general | solution.py:105
  117.9 2.9 %copy.83 = f32[8,128,512]{1,2,0:T(8,128)} copy(f32[8,128,512]{2,1,0:T(8,128)} %bitcast.274) | data formatting | bytes 4194304 | tf_op jit(solution)/shard_map/reshape | solution.py:127
  120.8 6.8 %convert_multiply_fusion = f32[1024,512]{1,0:T(8,128)} fusion(bf16[2048,512]{1,0:T(8,128)(2,1)} %param.22, bf16[1,1024,2048]{2,1,0:T(8,128)(2,1)} %all-gather.9.cloned.1.call-done), kind=kOutput, calls=%fused_computation.19 | convolution fusion | flops 2150629376 | bytes 8388608 | tf_op jit(solution)/shard_map/dot_general | solution.py:105
  127.6 2.9 %copy.105 = f32[1024,512]{0,1:T(8,128)} copy(f32[1024,512]{1,0:T(8,128)} %convert_multiply_fusion) | data formatting | bytes 4194304 | tf_op jit(solution)/shard_map/reshape | solution.py:193
  130.5 4.1 %exponential_multiply_fusion = (bf16[8,128,512]{1,2,0:T(8,128)(2,1)S(1)}, bf16[8,128,512]{1,2,0:T(8,128)(2,1)S(1)}, bf16[8,128,512]{1,2,0:T(8,128)(2,1)}) fusion(f32[8,128,512]{1,2,0:T(8,128)} %copy.83, f32[8,128,512]{1,2,0:T(8,128)} %copy-done.1, f32[8,512]{1,0:T(8,128)S(1)} %get-tuple-element.48, f32[8,128,512]{1,2,0:T(8,128)} %copy.78), kind=kLoop, calls=%fused_computation.72 | loop fusion | flops 4194304 | bytes 9453568 | tf_op jit(solution)/shard_map/mul | solution.py:161
  134.6 1.6 copy.91
  136.3 2.3 %reshape.477 = bf16[1024,4,128]{0,2,1:T(8,128)(2,1)} reshape(bf16[8,128,512]{1,0,2:T(8,128)(2,1)} %copy.91) | data formatting | bytes 2097152 | tf_op jit(solution)/shard_map/reshape | solution.py:161
  141.8 1.5 select_convert_fusion
  144.1 3.1 %fusion.148 = f32[8,4,128,128]{2,3,1,0:T(8,128)} fusion(bf16[8,4,128,128]{3,2,1,0:T(8,128)(2,1)} %get-tuple-element.47, bf16[8,128,4,128]{1,3,2,0:T(8,128)(2,1)S(1)} %bitcast.263), kind=kOutput, calls=%fused_computation.232 | convolution fusion | flops 134217728 | bytes 4194304 | tf_op jit(solution)/shard_map/bthd,bhde->bthe/dot_general | solution.py:159
  147.1 4.4 %add_bitcast_fusion = f32[8,128,4,128]{3,1,2,0:T(8,128)} fusion(f32[8,4,128,128]{2,3,1,0:T(8,128)} %fusion.148, bf16[8,128,4,128]{1,3,2,0:T(8,128)(2,1)S(1)} %bitcast.264, bf16[8,128,4,128]{1,3,2,0:T(8,128)(2,1)} %bitcast.269, f32[128,128]{1,0:T(8,128)} %fusion.114, bf16[8,128,4,128]{3,2,1,0:T(4,128)(2,1)} %copy-done.3), kind=kOutput, calls=%fused_computation.73 | convolution fusion | flops 270008320 | bytes 7405568 | tf_op jit(solution)/shard_map/bhts,bshe->bthe/dot_general | solution.py:133
  151.5 3.1 %copy.89 = f32[8,128,4,128]{3,1,0,2:T(8,128)} copy(f32[8,128,4,128]{3,1,2,0:T(8,128)} %add_bitcast_fusion) | data formatting | bytes 4194304 | tf_op jit(solution)/shard_map/add | solution.py:160
  154.7 3.0 %copy.94 = f32[1024,4,128]{0,2,1:T(8,128)} copy(f32[1024,4,128]{2,0,1:T(8,128)} %bitcast.266) | data formatting | bytes 4194304 | tf_op jit(solution)/shard_map/reshape | solution.py:160
  157.6 3.3 %multiply_reduce_fusion.1 = (f32[1024,4]{0,1:T(4,128)S(1)}, f32[1024,4,128]{0,2,1:T(8,128)S(1)}) fusion(f32[1024,4,128]{0,2,1:T(8,128)} %copy.94, bf16[1024,4,128]{0,2,1:T(8,128)(2,1)S(1)} %copy-done.8, bf16[4,128,128]{2,1,0:T(8,128)(2,1)} %bitcast.283, bf16[4,128,128]{2,1,0:T(8,128)(2,1)} %bitcast.282, f32[4,128,128]{2,1,0:T(8,128)} %bitcast.278, ...), kind=kOutput, calls=%fused_computation.71 | convolution fusion | flops 137621504 | bytes 6850568 | tf_op jit(solution)/shard_map/thd,hde->the/dot_general | solution.py:187
  161.8 6.2 %fusion.37 = bf16[1024,512]{1,0:T(8,128)(2,1)S(1)} fusion(bf16[1024,512]{1,0:T(8,128)(2,1)S(1)} %copy-done.7, f32[1039,512]{1,0:T(8,128)S(1)} %maximum_convert_fusion, f32[512]{0:T(512)S(1)} %copy-done.14, f32[1024]{0:T(1024)S(1)} %copy-done.13, pred[512]{0:T(512)(128)(4,1)S(1)} %copy-done.34, pred[512]{0:T(512)(128)(4,1)S(1)} %copy-done.35, ...), kind=kLoop, calls=%fused_computation.79 | loop fusion | flops 18874368 | bytes 35665920 | tf_op jit(solution)/shard_map/convert_element_type | solution.py:207
  168.9 2.4 %fusion.147 = f32[1024,2048]{1,0:T(8,128)S(1)} fusion(bf16[1024,512]{0,1:T(8,128)(2,1)S(1)} %fusion.34, bf16[512,2048]{1,0:T(8,128)(2,1)S(1)} %copy-done), kind=kOutput, calls=%fused_computation.231 | convolution fusion | flops 2147483648 | bytes 11534336 | tf_op jit(solution)/shard_map/dot_general | solution.py:218
  171.9 1.0 copy-done.10
  172.9 2.4 %convolution_add_fusion = f32[1024,2048]{1,0:T(8,128)S(1)} fusion(f32[1024,2048]{1,0:T(8,128)S(1)} %fusion.147, bf16[1024,512]{0,1:T(8,128)(2,1)S(1)} %bitcast.268, bf16[512,2048]{1,0:T(8,128)(2,1)S(1)} %copy-done.10), kind=kOutput, calls=%fused_computation.18 | convolution fusion | flops 2149580800 | bytes 19922944 | tf_op jit(solution)/shard_map/dot_general | solution.py:219
  175.4 1.7 copy.126
  177.0 17.0 %all_to_all.5 = f32[2,1024,1024]{1,2,0:T(8,128)} all-to-all(f32[2,1024,1024]{1,2,0:T(8,128)S(1)} %bitcast.262), channel_id=1, replica_groups=mesh['sp_0'=4,'sp_1'=4,'fs'=4,'tp'=2] {'tp'}, dimensions={0} | all-to-all | bytes 16777216 | tf_op jit(solution)/shard_map/all_to_all | solution.py:74
  194.0 6.7 %reduce_sum.55 = f32[1024,1024]{0,1:T(8,128)} reduce(f32[2,1024,1024]{1,2,0:T(8,128)} %all_to_all.5, f32[]{:T(128)} %constant.50.clone.1), dimensions={0}, to_apply=%region_3.4 | reduce | flops 1048576 | bytes 12582916 | tf_op jit(solution)/shard_map/reduce_sum | solution.py:75
  200.7 3.8 %fusion.62 = (f32[1024]{0:T(1024)S(1)}, f32[1024]{0:T(1024)S(1)}) fusion(f32[1024,1024]{0,1:T(8,128)} %reduce_sum.55, bf16[1,1024,1024]{2,1,0:T(8,128)(2,1)} %param.17), kind=kLoop, calls=%fused_computation.86 | loop fusion | flops 6289408 | bytes 6299648 | tf_op jit(solution)/shard_map/reduce_sum | solution.py:225
  204.5 1.8 all-gather.3
  206.4 1.8 all-gather.4
  208.3 4.4 %fusion.16 = bf16[1,1024,1024]{2,1,0:T(8,128)(2,1)} fusion(f32[1024]{0:T(1024)S(1)} %copy-done.16, f32[1024]{0:T(1024)S(1)} %copy-done.17, f32[1024]{0:T(1024)S(1)} %get-tuple-element.119, f32[1024]{0:T(1024)S(1)} %get-tuple-element.118, f32[1024,1024]{0,1:T(8,128)} %reduce_sum.55, bf16[1,1024,1024]{2,1,0:T(8,128)(2,1)} %param.17), kind=kLoop, calls=%fused_computation.29 | loop fusion | flops 8388608 | bytes 8404992 | tf_op jit(solution)/shard_map/broadcast_in_dim | solution.py:231
  (161 shorter events, 23.5 us)
Async XLA Ops:
  6.5 162.3 %copy-start = (bf16[512,2048]{1,0:T(8,128)(2,1)S(1)}, bf16[512,2048]{1,0:T(8,128)(2,1)}, u32[]{:S(2)}) copy-start(bf16[512,2048]{1,0:T(8,128)(2,1)} %param.28) | copy-start | bytes 6291460
  6.5 0.9 copy-start.12
  6.5 22.5 %all-gather.9.cloned.1.call-start = ((), (), s32[]{:S(2)}) async-start(), calls=%async_computation.1 | async-start | bytes 6291456 | tf_op jit(solution)/shard_map/all_gather | solution.py:103
  7.7 8.3 %copy-start.18 = (f32[512]{0:T(512)S(1)}, f32[512]{0:T(512)}, u32[]{:S(2)}) copy-start(f32[512]{0:T(512)} %param.25) | copy-start | bytes 6148
  34.2 1.0 copy-start.6
  42.7 19.2 %copy-start.3 = (bf16[8,128,4,128]{3,2,1,0:T(4,128)(2,1)}, bf16[8,128,4,128]{3,2,1,0:T(4,128)(2,1)S(1)}, u32[]{:S(2)}) copy-start(bf16[8,128,4,128]{3,2,1,0:T(4,128)(2,1)S(1)} %reshape.465) | copy-start | bytes 3145732
  59.2 2.0 copy-start.2
  59.7 2.3 %copy-start.1 = (f32[8,128,512]{1,2,0:T(8,128)}, f32[8,128,512]{1,2,0:T(8,128)S(1)}, u32[]{:S(2)}) copy-start(f32[8,128,512]{1,2,0:T(8,128)S(1)} %fusion.38) | copy-start | bytes 6291460
  63.8 15.4 %copy-start.20 = (bf16[1,128]{1,0:T(2,128)(2,1)S(1)}, bf16[1,128]{1,0:T(2,128)(2,1)}, u32[]{:S(2)}) copy-start(bf16[1,128]{1,0:T(2,128)(2,1)} %constant.36.clone.1) | copy-start | bytes 772
  90.7 20.8 %copy-start.5 = (bf16[4,577,128]{2,1,0:T(8,128)(2,1)}, bf16[4,577,128]{2,1,0:T(8,128)(2,1)S(1)}, u32[]{:S(2)}) copy-start(bf16[4,577,128]{2,1,0:T(8,128)(2,1)S(1)} %all-gather.5) | copy-start | bytes 1772548
  97.5 14.8 %copy-start.38 = (bf16[1,1024,2048]{2,1,0:T(8,128)(2,1)S(1)}, bf16[1,1024,2048]{2,1,0:T(8,128)(2,1)}, u32[]{:S(2)}) copy-start(bf16[1,1024,2048]{2,1,0:T(8,128)(2,1)} %all-gather.9.cloned.1.call-done) | copy-start | bytes 12582916
  108.9 1.8 copy-start.9
  134.6 4.0 %copy-start.15 = (bf16[4,1,128]{2,1,0:T(2,128)(2,1)S(1)}, bf16[4,1,128]{2,1,0:T(2,128)(2,1)}, u32[]{:S(2)}) copy-start(bf16[4,1,128]{2,1,0:T(2,128)(2,1)} %slice.279) | copy-start | bytes 3076
  154.7 3.0 %copy-start.8 = (bf16[1024,4,128]{0,2,1:T(8,128)(2,1)S(1)}, bf16[1024,4,128]{0,2,1:T(8,128)(2,1)}, u32[]{:S(2)}) copy-start(bf16[1024,4,128]{0,2,1:T(8,128)(2,1)} %reshape.477) | copy-start | bytes 3145732
  157.6 3.5 %copy-start.7 = (bf16[1024,512]{1,0:T(8,128)(2,1)S(1)}, bf16[1024,512]{1,0:T(8,128)(2,1)}, u32[]{:S(2)}) copy-start(bf16[1024,512]{1,0:T(8,128)(2,1)} %copy-done.6) | copy-start | bytes 3145732
  161.0 0.7 copy-start.13
  161.0 0.7 copy-start.14
  161.0 0.7 copy-start.22
  161.0 0.7 copy-start.23
  161.0 0.7 copy-start.24
  161.0 0.7 copy-start.25
  161.0 0.6 copy-start.26
  161.0 0.6 copy-start.27
  161.0 0.6 copy-start.28
  161.1 0.6 copy-start.29
  161.1 0.7 copy-start.30
  161.1 0.7 copy-start.31
  161.1 0.7 copy-start.32
  161.1 0.7 copy-start.33
  161.1 0.7 copy-start.34
  161.1 0.7 copy-start.35
  161.1 0.7 copy-start.36
  161.1 0.7 copy-start.37
  161.8 6.2 %copy-start.11 = (bf16[2,256,256]{2,1,0:T(8,128)(2,1)S(1)}, bf16[2,256,256]{2,1,0:T(8,128)(2,1)}, u32[]{:S(2)}) copy-start(bf16[2,256,256]{2,1,0:T(8,128)(2,1)} %param.23) | copy-start | bytes 786436
  168.0 0.7 copy-start.19
  168.8 2.4 %copy-start.4 = (f32[1024,512]{0,1:T(8,128)S(1)}, f32[1024,512]{0,1:T(8,128)}, u32[]{:S(2)}) copy-start(f32[1024,512]{0,1:T(8,128)} %copy.105) | copy-start | bytes 6291460
  168.9 2.4 %copy-start.21 = (f32[128]{0:T(128)S(1)}, f32[128]{0:T(128)}, u32[]{:S(2)}) copy-start(f32[128]{0:T(128)} %param.27) | copy-start | bytes 1540
  171.3 1.6 copy-start.10
  200.7 7.6 %copy-start.16 = (f32[1024]{0:T(1024)S(1)}, f32[1024]{0:T(1024)}, u32[]{:S(2)}) copy-start(f32[1024]{0:T(1024)} %param.31) | copy-start | bytes 12292
  200.7 7.6 %copy-start.17 = (f32[1024]{0:T(1024)S(1)}, f32[1024]{0:T(1024)}, u32[]{:S(2)}) copy-start(f32[1024]{0:T(1024)} %param.30) | copy-start | bytes 12292
Sparse Core Ops, SparseCore 0:
  9.0 19.9 all-gather.8
where the time goes:
time: 221 us; the launch traced here: 220 us
  other arithmetic  55.6 us (25%)
  matrix products  50.2 us (23%)
  blocking collectives  43.1 us (20%)
  local copies, waits for them, and re-layouts  35 us (16%)
  between operations  21.6 us (10%)
  waiting for transfers between devices  13.8 us (6%)
    dot_general x5, matrix products, local(): jnp.dot(column_piece, weight, preferred_element_type=jnp.float32)  31.9 us
    all_gather x2, blocking collectives, gathered_once(): both, at, found = (lax.all_gather(jnp.concatenate(lines), axis), 0, {})  22.4 us
    all_to_all x1, blocking collectives, summed_on_arrival(): pieces = lax.all_to_all(split_up(x, dim, devices), axis, 0, 0, tiled=True)  17 us
    all_gather x1, waiting for transfers between devices, local(): column_piece = lax.all_gather(features, 'tp', axis=1, tiled=True)  13.1 us
    add x8, other arithmetic, block_step(): jnp.exp(end_blk).reshape(heads_here, DK)[:, :, None] * state + term_blk  8.93 us
    reduce_sum x1, other arithmetic, summed_on_arrival(): return jnp.sum(pieces, axis=0)  6.73 us
    convert_element_type x1, other arithmetic, local(): (window_sum / counts - pooled.astype(jnp.float32)).astype(jnp.bfloat16)  6.16 us
    dynamic_update_slice x8, other arithmetic, local(): lax.scan(block_step, start_carry, (log_end, own_terms))  5.44 us
  transfers between devices with their start and end apart: 1, of which 1 were waited for; matrix products, arithmetic and copies ran while one was open for 4% of the time, Pallas kernels for 0%

commit v1 on v0

v1 whole, which is shorter than its diff:
```python
import functools

import jax
import jax.numpy as jnp
from jax import lax
from jax.experimental import pallas as pl
from jax.experimental.pallas import tpu as pltpu
from jax.sharding import Mesh
from jax.sharding import PartitionSpec as P

BF16 = jnp.bfloat16
F32 = jnp.float32
MESH = pl.DeviceIdType.MESH

ALPHA = 2.0**0.25
EPS_RMS = 1e-06
EPS_NORM = 1e-05

T = 1024
H = 1024
C = 512
DK = 128
NH = C // DK
B = 128
NB = T // B
R = 256
NT = T // R
NX = 4
MSG = DK + 16


def dot(a, b):
    return jnp.dot(a, b, preferred_element_type=F32)


def dot_tn(a, b):
    return lax.dot_general(a, b, (((0,), (0,)), ((), ())), preferred_element_type=F32)


def dot_nt(a, b):
    return lax.dot_general(a, b, (((1,), (1,)), ((), ())), preferred_element_type=F32)


def sigmoid(x):
    return 1.0 / (1.0 + jnp.exp(-x))


def split_rows(row):
    hi = row.astype(BF16)
    rest = row - hi.astype(F32)
    mid = rest.astype(BF16)
    low = (rest - mid.astype(F32)).astype(BF16)
    rows = lax.broadcasted_iota(jnp.int32, (16, DK), 0)
    return jnp.where(
        rows == 0,
        hi.astype(F32),
        jnp.where(rows == 1, mid.astype(F32), jnp.where(rows == 2, low.astype(F32), 0.0)),
    ).astype(BF16)


def joined_rows(block):
    return jnp.sum(block.astype(F32), axis=0, keepdims=True)


def kernel(
    nz,
    stream, wp, wq, wf, wv, wg, pmix, pscale, lbound, edecay, rgain, wop, wor, ngain, nbias,
    out,
    x_v, wf_v, wv_v, wp_v, wq_v, wg_v, wo_v,
    pmix_v, pscale_v, lb_v, ed_v, rgain_v, ngain_v, nbias_v,
    v_v, explog_v, down_v, pooled_v, halo_v, sq_v, gate_v, a_v,
    st_v, cur_v, off_v, offcur_v, band_v, tri_v,
    s1_send, s1_recv, s2_send, s2_recv, s3_send, s3_recv, pre_v, bsum_v,
    resid_v, stat_v, ostat_v, o_v,
    load_sem, param_sem,
    xs_sem, xr_sem, ws_sem, wr_sem, ps_sem, pr_sem, rs_sem, rr_sem, ss_sem, sr_sem,
    hs_sem, hr_sem, m1s_sem, m1r_sem, m2s_sem, m2r_sem, m3s_sem, m3r_sem, o_sem,
):
    z = lax.axis_index("sp_0")
    x = lax.axis_index("sp_1")
    tp = lax.axis_index("tp")
    sp = z * NX + x
    other = 1 - tp
    n_sp = nz * NX
    after = lax.rem(sp + 1, n_sp)
    prior = lax.rem(sp + n_sp - 1, n_sp)
    partner = {"tp": other}
    x_peers = [{"sp_1": lax.rem(x + d, NX)} for d in range(1, NX)]
    z_peers = [{"sp_0": lax.rem(z + d, nz)} for d in range(1, nz)]
    next_dev = {"sp_0": after // NX, "sp_1": lax.rem(after, NX)}
    prev_dev = {"sp_0": prior // NX, "sp_1": lax.rem(prior, NX)}

    own_rows = pl.ds(pl.multiple_of(tp * H, H), H)
    oth_rows = pl.ds(pl.multiple_of(other * H, H), H)

    def load_tile(c):
        rows = pl.ds(c * R, R)
        return pltpu.make_async_copy(stream.at[rows, :], x_v.at[rows, pl.ds(0, H)], load_sem.at[c])

    loads = [load_tile(c) for c in range(NT)]
    weight_loads = []
    for k, (src, dst) in enumerate(((wf, wf_v), (wv, wv_v), (wp, wp_v), (wq, wq_v), (wg, wg_v))):
        weight_loads.append(
            (
                pltpu.make_async_copy(src.at[own_rows, :], dst.at[pl.ds(0, H), :], load_sem.at[NT + 2 * k]),
                pltpu.make_async_copy(src.at[oth_rows, :], dst.at[pl.ds(H, H), :], load_sem.at[NT + 2 * k + 1]),
            )
        )
    params = [
        pltpu.make_async_copy(src, dst, param_sem.at[k])
        for k, (src, dst) in enumerate(
            (
                (lbound, lb_v), (edecay, ed_v), (pmix, pmix_v), (pscale, pscale_v),
                (rgain, rgain_v), (ngain, ngain_v), (nbias, nbias_v),
            )
        )
    ]
    own_cols = pl.ds(pl.multiple_of(tp * H, H), H)
    oth_cols = pl.ds(pl.multiple_of(other * H, H), H)
    out_loads = [
        pltpu.make_async_copy(src.at[:, own_cols], wo_v.at[pl.ds(k * C, C), :], load_sem.at[NT + 10 + k])
        for k, src in enumerate((wop, wor))
    ]
    loads[0].start()
    weight_loads[0][0].start()
    weight_loads[0][1].start()
    params[0].start()
    params[1].start()
    for c in range(1, NT):
        loads[c].start()
    for pair in weight_loads[1:]:
        pair[0].start()
        pair[1].start()
    for k in range(2, 7):
        params[k].start()
    for c in out_loads:
        c.start()

    barrier = pltpu.get_barrier_semaphore()
    greeted = [partner] + x_peers + z_peers + [next_dev, prev_dev]
    for dev in greeted:
        pl.semaphore_signal(barrier, inc=1, device_id=dev, device_id_type=MESH)
    pl.semaphore_wait(barrier, len(greeted))

    def send(src, dst, s_sem, r_sem, dev):
        return pltpu.make_async_remote_copy(
            src_ref=src, dst_ref=dst, send_sem=s_sem, recv_sem=r_sem, device_id=dev, device_id_type=MESH
        )

    x_sends = [
        send(
            stream.at[pl.ds(c * R, R), :], x_v.at[pl.ds(c * R, R), pl.ds(H, H)],
            xs_sem.at[c], xr_sem.at[c], partner,
        )
        for c in range(NT)
    ]
    for c in x_sends:
        c.start()
    w_sends = [
        send(src.at[:, oth_cols], wo_v.at[pl.ds((2 + k) * C, C), :], ws_sem.at[k], wr_sem.at[k], partner)
        for k, src in enumerate((wop, wor))
    ]
    for c in w_sends:
        c.start()

    row = lax.broadcasted_iota(jnp.int32, (B, B), 0)
    col = lax.broadcasted_iota(jnp.int32, (B, B), 1)
    lower = row >= col
    tri_v[...] = jnp.where(lower, 1.0, 0.0).astype(BF16)
    brow = lax.broadcasted_iota(jnp.int32, (B, 2 * B), 0)
    lag = brow + B - lax.broadcasted_iota(jnp.int32, (B, 2 * B), 1)
    for g in range(2):
        width = jnp.left_shift(2, 2 * tp + g)
        band_v[g] = jnp.where((lag >= 0) & (lag < width), 1.0, 0.0).astype(BF16)
    cur_v[...] = jnp.zeros_like(cur_v)
    offcur_v[...] = jnp.zeros_like(offcur_v)

    params[0].wait()
    params[1].wait()
    weight_loads[0][0].wait()
    weight_loads[0][1].wait()
    weight_loads[1][0].wait()
    weight_loads[1][1].wait()
    for c in range(NT):
        loads[c].wait()
    for c in range(NT):
        x_sends[c].wait_recv()

    @pl.loop(0, NT)
    def _(c):
        r0 = pl.multiple_of(c * R, R)
        xt = x_v[pl.ds(r0, R), :]
        fi = dot(xt, wf_v[...]).astype(BF16).astype(F32)
        vi = dot(xt, wv_v[...]).astype(BF16)
        v_v[pl.ds(r0, R), :] = vi
        gap = 1.0 - lb_v[...]
        w_in = gap * sigmoid(-fi)
        keep = jnp.log(1.0 - w_in)
        for s in range(R // B):
            b = c * (R // B) + s
            rb = pl.multiple_of(r0 + s * B, B)
            rows = slice(s * B, (s + 1) * B)
            ed = ed_v[pl.ds(rb, B), :]
            tri = tri_v[...]
            off = offcur_v[...]
            ends = []
            for h in range(NH):
                hs = slice(h * DK, (h + 1) * DK)
                lk = keep[rows, hs] + ed[:, h : h + 1]
                hi = lk.astype(BF16)
                lo = (lk - hi.astype(F32)).astype(BF16)
                total = dot(tri, hi) + dot(tri, lo)
                end = total[B - 1 : B, :]
                ends.append(end)
                wi = w_in[rows, hs]
                explog_v[pl.ds(rb, B), hs] = jnp.exp(total)
                down_v[pl.ds(rb, B), hs] = (wi * jnp.exp(-total)).astype(BF16)
                inw = (wi * jnp.exp(end - total)).astype(BF16)
                own = dot_tn(vi[rows, hs], inw)
                st = cur_v[h]
                st_v[b, h] = st
                cur_v[h] = jnp.exp(end) * st + own
            off_v[b] = off
            offcur_v[...] = off + jnp.concatenate(ends, axis=1)

    for h in range(NH):
        s1_send[h, pl.ds(0, DK), :] = cur_v[h].astype(BF16)
        s1_send[h, pl.ds(DK, 16), :] = split_rows(offcur_v[0:1, h * DK : (h + 1) * DK])

    def msg1(d):
        to = lax.rem(x + d, NX)
        return send(s1_send.at[to], s1_recv.at[x], m1s_sem.at[d - 1], m1r_sem.at[x], {"sp_1": to})

    def arrival1(d):
        frm = lax.rem(x + d, NX)
        return send(s1_send.at[frm], s1_recv.at[frm], m1s_sem.at[d - 1], m1r_sem.at[frm], {"sp_1": frm})

    for d in range(1, NX):
        msg1(d).start()

    weight_loads[2][0].wait()
    weight_loads[2][1].wait()
    pooled_v[pl.ds(0, B), :] = jnp.zeros((B, C), BF16)

    @pl.loop(0, NT)
    def _(c):
        r0 = pl.multiple_of(c * R, R)
        pooled_v[pl.ds(pl.multiple_of(r0 + B, B), R), :] = dot(
            x_v[pl.ds(r0, R), :], wp_v[...]
        ).astype(BF16)

    halo = send(pooled_v.at[pl.ds(T + B - 16, 16), :], halo_v, hs_sem, hr_sem, next_dev)
    halo.start()

    s1_recv[x] = s1_send[x]
    for d in range(1, NX):
        arrival1(d).wait_recv()
    run = jnp.zeros((DK, DK), F32)
    logs = jnp.zeros((1, DK), F32)
    for k in range(NX):
        pre_v[k] = run
        bsum_v[k] = jnp.broadcast_to(logs, (8, DK))
        a_k = joined_rows(s1_recv[k, pl.ds(DK, 16), :])
        run = jnp.exp(a_k) * run + s1_recv[k, pl.ds(0, DK), :].astype(F32)
        logs = logs + a_k
    s2_send[pl.ds(0, DK), :] = run.astype(BF16)
    s2_send[pl.ds(DK, 16), :] = split_rows(logs)

    def msg2(d):
        to = lax.rem(z + d, nz)
        return send(s2_send, s2_recv.at[z], m2s_sem.at[d - 1], m2r_sem.at[z], {"sp_0": to})

    def arrival2(d):
        frm = lax.rem(z + d, nz)
        return send(s2_send, s2_recv.at[frm], m2s_sem.at[d - 1], m2r_sem.at[frm], {"sp_0": frm})

    for d in range(1, nz):
        msg2(d).start()

    weight_loads[3][0].wait()
    weight_loads[3][1].wait()

    @pl.loop(0, NT)
    def _(c):
        r0 = pl.multiple_of(c * R, R)
        q = dot(x_v[pl.ds(r0, R), :], wq_v[...]).astype(BF16).astype(F32)
        q = q * sigmoid(q)
        up = (q * explog_v[pl.ds(r0, R), :]).astype(BF16)
        for s in range(R // B):
            rb = pl.multiple_of(r0 + s * B, B)
            for h in range(NH):
                hs = slice(h * DK, (h + 1) * DK)
                u = up[s * B : (s + 1) * B, hs]
                sc = dot_nt(u, down_v[pl.ds(rb, B), hs])
                sc = jnp.where(lower, sc, 0.0).astype(BF16)
                sq_v[pl.ds(rb, B), 2 * h * DK : (2 * h + 1) * DK] = sc
                sq_v[pl.ds(rb, B), (2 * h + 1) * DK : (2 * h + 2) * DK] = u

    s2_recv[z] = s2_send[...]
    for d in range(1, nz):
        arrival2(d).wait_recv()
    run = jnp.zeros((DK, DK), F32)
    for k in range(nz - 1):
        b_k = joined_rows(s2_recv[k, pl.ds(DK, 16), :])
        new = jnp.exp(b_k) * run + s2_recv[k, pl.ds(0, DK), :].astype(F32)
        run = jnp.where(k < z, new, run)
    for k in range(NX):
        s3_send[k] = (jnp.exp(bsum_v[k][0:1, :]) * run + pre_v[k]).astype(BF16)

    def msg3(d):
        to = lax.rem(x + d, NX)
        return send(s3_send.at[to], s3_recv.at[x], m3s_sem.at[d - 1], m3r_sem.at[x], {"sp_1": to})

    def arrival3(d):
        frm = lax.rem(x + d, NX)
        return send(s3_send.at[frm], s3_recv.at[frm], m3s_sem.at[d - 1], m3r_sem.at[frm], {"sp_1": frm})

    for d in range(1, NX):
        msg3(d).start()

    weight_loads[4][0].wait()
    weight_loads[4][1].wait()
    for k in range(2, 7):
        params[k].wait()

    @pl.loop(0, NT)
    def _(c):
        r0 = pl.multiple_of(c * R, R)
        g = dot(x_v[pl.ds(r0, R), :], wg_v[...]).astype(BF16).astype(F32)
        gain = jnp.concatenate([rgain_v[...]] * NH, axis=1)
        gate_v[pl.ds(r0, R), :] = g * sigmoid(g) * gain

    halo.wait_recv()
    pooled_v[pl.ds(B - 16, 16), :] = jnp.where(sp > 0, halo_v[...], jnp.zeros_like(halo_v))

    def pool_send(c):
        rows = pl.ds(pl.multiple_of(c * R, R), R)
        return send(a_v.at[rows, pl.ds(0, C)], a_v.at[rows, pl.ds(2 * C, C)], ps_sem.at[c], pr_sem.at[c], partner)

    @pl.loop(0, NT)
    def _(c):
        r0 = pl.multiple_of(c * R, R)
        for s in range(R // B):
            rb = pl.multiple_of(r0 + s * B, B)
            position = sp * T + rb + lax.broadcasted_iota(jnp.int32, (B, 1), 0) + 1
            for g in range(2):
                cols = slice(g * 256, (g + 1) * 256)
                total = dot(band_v[g], pooled_v[pl.ds(rb, 2 * B), cols])
                here = pooled_v[pl.ds(pl.multiple_of(rb + B, B), B), cols].astype(F32)
                width = jnp.left_shift(2, 2 * tp + g)
                count = jnp.minimum(position, width).astype(F32)
                diff = (total / count - here).astype(BF16)
                mixed = dot(diff, pmix_v[g]) * pscale_v[:, cols]
                a_v[pl.ds(rb, B), cols] = mixed.astype(BF16)

    for c in range(NT):
        pool_send(c).start()

    s3_recv[x] = s3_send[x]
    for d in range(1, NX):
        arrival3(d).wait_recv()

    for c in out_loads:
        c.wait()
    for c in w_sends:
        c.wait_recv()
    for c in range(NT):
        pool_send(c).wait_recv()

    def rec_send(c):
        rows = pl.ds(pl.multiple_of(c * R, R), R)
        return send(a_v.at[rows, pl.ds(C, C)], a_v.at[rows, pl.ds(3 * C, C)], rs_sem.at[c], rr_sem.at[c], partner)

    def stat_send(c):
        rows = pl.ds(pl.multiple_of(c * R, R), R)
        return send(stat_v.at[rows, :], ostat_v.at[rows, :], ss_sem.at[c], sr_sem.at[c], partner)

    @pl.loop(0, NT)
    def _(c):
        r0 = pl.multiple_of(c * R, R)
        for s in range(R // B):
            b = c * (R // B) + s
            rb = pl.multiple_of(r0 + s * B, B)
            far = jnp.exp(off_v[b])
            for h in range(NH):
                hs = slice(h * DK, (h + 1) * DK)
                state = st_v[b, h] + far[:, hs] * s3_recv[h].astype(F32)
                raw = dot(sq_v[pl.ds(rb, B), 2 * h * DK : (2 * h + 1) * DK], v_v[pl.ds(rb, B), hs])
                raw = raw + dot_nt(
                    sq_v[pl.ds(rb, B), (2 * h + 1) * DK : (2 * h + 2) * DK], state.astype(BF16)
                )
                power = jnp.mean(raw * raw, axis=1, keepdims=True)
                normed = raw * lax.rsqrt(power + EPS_RMS) * gate_v[pl.ds(rb, B), hs]
                a_v[pl.ds(rb, B), C + h * DK : C + (h + 1) * DK] = normed.astype(BF16)
        rec_send(c).start()

    @pl.loop(0, NT)
    def _(c):
        r0 = pl.multiple_of(c * R, R)
        rec_send(c).wait_recv()
        mix = dot(a_v[pl.ds(r0, R), :], wo_v[...])
        resid = ALPHA * x_v[pl.ds(r0, R), 0:H].astype(F32) + mix
        resid_v[pl.ds(r0, R), :] = resid
        mean = jnp.sum(resid, axis=1, keepdims=True) * (1.0 / H)
        dev = resid - mean
        m2 = jnp.sum(dev * dev, axis=1, keepdims=True)
        lane = lax.broadcasted_iota(jnp.int32, (R, DK), 1)
        stat_v[pl.ds(r0, R), :] = jnp.where(lane == 0, mean, m2)
        stat_send(c).start()

    def out_copy(c):
        rows = pl.ds(pl.multiple_of(c * R, R), R)
        return pltpu.make_async_copy(o_v.at[rows, :], out.at[rows, :], o_sem.at[c])

    @pl.loop(0, NT)
    def _(c):
        r0 = pl.multiple_of(c * R, R)
        stat_send(c).wait_recv()
        mine = stat_v[pl.ds(r0, R), :]
        theirs = ostat_v[pl.ds(r0, R), :]
        gap = mine[:, 0:1] - theirs[:, 0:1]
        mean = 0.5 * (mine[:, 0:1] + theirs[:, 0:1])
        var = (mine[:, 1:2] + theirs[:, 1:2] + gap * gap * (0.5 * H)) * (1.0 / (2 * H))
        scale = lax.rsqrt(var + EPS_NORM)
        o_v[pl.ds(r0, R), :] = (
            (resid_v[pl.ds(r0, R), :] - mean) * scale * ngain_v[...] + nbias_v[...]
        ).astype(BF16)
        out_copy(c).start()

    for c in range(NT):
        out_copy(c).wait()
        x_sends[c].wait_send()
        pool_send(c).wait_send()
        rec_send(c).wait_send()
        stat_send(c).wait_send()
    for c in w_sends:
        c.wait_send()
    halo.wait_send()
    for d in range(1, NX):
        msg1(d).wait_send()
        msg3(d).wait_send()
    for d in range(1, nz):
        msg2(d).wait_send()


def layer(nz, *args):
    (stream, wp, wq, wf, wv, wg, pmix, pscale, lb, ed, rgain, wop, wor, ngain, nbias) = args
    anyspace = pl.BlockSpec(memory_space=pl.ANY)
    sem = pltpu.SemaphoreType.DMA
    scratch = [
        pltpu.VMEM((T, 2 * H), BF16),
        *[pltpu.VMEM((2 * H, C), BF16)] * 5,
        pltpu.VMEM((4 * C, H), BF16),
        pltpu.VMEM((2, 256, 256), BF16),
        pltpu.VMEM((1, C), F32),
        pltpu.VMEM((1, C), F32),
        pltpu.VMEM((T, NH), F32),
        pltpu.VMEM((1, DK), F32),
        pltpu.VMEM((1, H), F32),
        pltpu.VMEM((1, H), F32),
        pltpu.VMEM((T, C), BF16),
        pltpu.VMEM((T, C), F32),
        pltpu.VMEM((T, C), BF16),
        pltpu.VMEM((T + B, C), BF16),
        pltpu.VMEM((16, C), BF16),
        pltpu.VMEM((T, 2 * C), BF16),
        pltpu.VMEM((T, C), F32),
        pltpu.VMEM((T, 4 * C), BF16),
        pltpu.VMEM((NB, NH, DK, DK), F32),
        pltpu.VMEM((NH, DK, DK), F32),
        pltpu.VMEM((NB, 1, C), F32),
        pltpu.VMEM((1, C), F32),
        pltpu.VMEM((2, B, 2 * B), BF16),
        pltpu.VMEM((B, B), BF16),
        pltpu.VMEM((NH, MSG, DK), BF16),
        pltpu.VMEM((NX, MSG, DK), BF16),
        pltpu.VMEM((MSG, DK), BF16),
        pltpu.VMEM((nz, MSG, DK), BF16),
        pltpu.VMEM((NX, DK, DK), BF16),
        pltpu.VMEM((NX, DK, DK), BF16),
        pltpu.VMEM((NX, DK, DK), F32),
        pltpu.VMEM((NX, 8, DK), F32),
        pltpu.VMEM((T, H), F32),
        pltpu.VMEM((T, DK), F32),
        pltpu.VMEM((T, DK), F32),
        pltpu.VMEM((T, H), BF16),
        sem((NT + 12,)), sem((7,)),
        sem((NT,)), sem((NT,)), sem((2,)), sem((2,)), sem((NT,)), sem((NT,)),
        sem((NT,)), sem((NT,)), sem((NT,)), sem((NT,)),
        sem, sem,
        sem((NX - 1,)), sem((NX,)), sem((nz - 1,)), sem((nz,)), sem((NX - 1,)), sem((NX,)),
        sem((NT,)),
    ]
    result = pl.pallas_call(
        functools.partial(kernel, nz),
        out_shape=jax.ShapeDtypeStruct((T, H), BF16),
        in_specs=[anyspace] * 15,
        out_specs=anyspace,
        scratch_shapes=scratch,
        compiler_params=pltpu.CompilerParams(
            collective_id=0, has_side_effects=True, vmem_limit_bytes=66_000_000
        ),
    )(
        stream[0], wp, wq, wf, wv, wg, pmix,
        pscale.reshape(1, C), lb.reshape(1, C), ed, rgain.reshape(1, DK),
        wop, wor, ngain.reshape(1, H), nbias.reshape(1, H),
    )
    return result[None]


def solution(mesh):
    devices = mesh.devices
    nz = devices.shape[0] // NX
    torus = Mesh(
        devices.reshape(nz, NX, mesh.shape["fs"], mesh.shape["tp"]), ("sp_0", "sp_1", "fs", "tp")
    )
    sp = ("sp_0", "sp_1")
    cols = P(None, "tp")
    return jax.shard_map(
        functools.partial(layer, nz),
        mesh=torus,
        in_specs=(
            P("fs", sp, "tp"), cols, cols, cols, cols, cols,
            P("tp", None, None), P("tp"), P("tp"), P(sp, "tp"), P(),
            P("tp", None), P("tp", None), P("tp"), P("tp"),
        ),
        out_specs=P("fs", sp, "tp"),
        check_vma=False,
    )
```

time: 221 us -> 53.5 us (0.24)
  other arithmetic: 55.6 us -> 0 us
  matrix products: 50.2 us -> 0 us
  Pallas kernels: 0 us -> 48.5 us
  blocking collectives: 43.1 us -> 0 us
  local copies, waits for them, and re-layouts: 35 us -> 4.82 us
  between operations: 21.6 us -> 0.01 us
  waiting for transfers between devices: 13.8 us -> 0 us
    dot_general x13 -> x0, matrix products: 50.2 us -> none  [the longest x5 31.9 us: local(): jnp.dot(column_piece, weight, preferred_element_type=jnp.float32)]
    pallas_call x0 -> x1, Pallas kernels: none -> 48.5 us  [layer(): pl.pallas_call(functools.partial(kernel, nz), out_shape=jax.ShapeDtypeStr...]
    all_gather x4 -> x0, blocking collectives: 26.1 us -> none  [the longest x2 22.4 us: gathered_once(): both, at, found = (lax.all_gather(jnp.concatenate(lines), axis), 0, {})]
    reshape x10 -> x0, local copies, waits for them, and re-layouts: 20 us -> none  [the longest x1 2.97 us: local(): local_out = (inside + carried).reshape(length, heads_here, DK)]
    all_to_all x1 -> x0, blocking collectives: 17 us -> none  [summed_on_arrival(): pieces = lax.all_to_all(split_up(x, dim, devices), axis, 0, 0, tiled=True)]
    convert_element_type x16 -> x0, other arithmetic: 13.8 us -> none  [the longest x1 6.16 us: local(): (window_sum / counts - pooled.astype(jnp.float32)).astype(jnp.bfloat16)]
    all_gather x1 -> x0, waiting for transfers between devices: 13.1 us -> none  [local(): column_piece = lax.all_gather(features, 'tp', axis=1, tiled=True)]
    add x17 -> x0, other arithmetic: 11.5 us -> none  [the longest x8 8.93 us: block_step(): jnp.exp(end_blk).reshape(heads_here, DK)[:, :, None] * state + term_blk]
  transfers between devices with their start and end apart: 1 -> 0, of which waited for: 1 -> 0; matrix products, arithmetic and copies ran while one was open for 4% -> 0% of each run, Pallas kernels for 0% -> 0%
where the time goes in v1:
time: 53.5 us; the launch traced here: 53.3 us
  Pallas kernels  48.5 us (91%)
  local copies, waits for them, and re-layouts  4.82 us (9%)
    pallas_call x1, Pallas kernels, layer(): pl.pallas_call(functools.partial(kernel, nz), out_shape=jax.ShapeDtypeStr...  48.5 us
    unnamed x2, local copies, waits for them, and re-layouts  4.82 us

profile of v1, /device:TPU:1, one launch (start us, length us, event | category | flops | bytes accessed | tf_op | source)
XLA Modules:
  0.0 53.3 jit_solution(5901354957630190103)
XLA Ops:
  0.0 1.7 %copy.16.edecay = f32[1024,4]{1,0:T(8,128)} copy(f32[1024,4]{0,1:T(4,128)} %param.24) | data formatting | bytes 32768 | tf_op args[9]
  1.7 48.5 %shard_map.145 = bf16[1024,1024]{1,0:T(8,128)(2,1)} custom-call(bf16[1024,1024]{1,0:T(8,128)(2,1)} %bitcast.8, bf16[2048,512]{1,0:T(8,128)(2,1)} %wp.1, bf16[2048,512]{1,0:T(8,128)(2,1)} %wq.1, bf16[2048,512]{1,0:T(8,128)(2,1)} %wf.1, bf16[2048,512]{1,0:T(8,128)(2,1)} %wv.1, bf16[2048,512]{1,0:T(8,128)(2,1)} %wg.1, bf16[2,256,256]{2,1,0:T(8,128)(2,1)} %pmix.1, ...), custom_call_target="tpu_custom_call" | custom-call | tf_op jit(solution)/shard_map/pallas_call | solution.py:494
  50.2 3.1 %copy.18 = bf16[1,1024,1024]{2,1,0:T(8,128)(2,1)} copy(bf16[1,1024,1024]{2,1,0:T(8,128)(2,1)} %bitcast.7) | data formatting | bytes 4194304

commit v2 on v1

v2 whole, which is shorter than its diff:
```python
import functools
import math

import jax
import jax.numpy as jnp
from jax import lax
from jax.experimental import pallas as pl
from jax.experimental.pallas import tpu as pltpu
from jax.sharding import Mesh
from jax.sharding import PartitionSpec as P

BF16 = jnp.bfloat16
F32 = jnp.float32
MESH = pl.DeviceIdType.MESH

ALPHA = 2.0**0.25
EPS_RMS = 1e-06
EPS_NORM = 1e-05
LOG2E = math.log2(math.e)

T = 1024
H = 1024
C = 512
DK = 128
NH = C // DK
B = 128
NB = T // B
R = 256
NT = T // R
NX = 4
MSG = DK + 16


def dot(a, b):
    return jnp.dot(a, b, preferred_element_type=F32)


def dot_tn(a, b):
    return lax.dot_general(a, b, (((0,), (0,)), ((), ())), preferred_element_type=F32)


def dot_nt(a, b):
    return lax.dot_general(a, b, (((1,), (1,)), ((), ())), preferred_element_type=F32)


def silu(x):
    half = 0.5 * x
    return half + half * jnp.tanh(half)


def split_rows(row):
    hi = row.astype(BF16)
    rest = row - hi.astype(F32)
    mid = rest.astype(BF16)
    low = (rest - mid.astype(F32)).astype(BF16)
    rows = lax.broadcasted_iota(jnp.int32, (16, DK), 0)
    return jnp.where(
        rows == 0,
        hi.astype(F32),
        jnp.where(rows == 1, mid.astype(F32), jnp.where(rows == 2, low.astype(F32), 0.0)),
    ).astype(BF16)


def joined_rows(block):
    return jnp.sum(block.astype(F32), axis=0, keepdims=True)


def kernel(
    nz,
    stream, wp, wq, wf, wv, wg, pmix, pscale, lbound, edecay, rgain, wop, wor, ngain, nbias,
    out,
    x_v, wf_v, wv_v, wp_v, wq_v, wg_v, wo_v,
    pmix_v, pscale_v, lb_v, ed_v, edc_v, rgain_v, ngain_v, nbias_v,
    f_v, v_v, explog_v, down_v, pooled_v, halo_v, sq_v, gate_v, a_v,
    st_v, cur_v, off_v, offcur_v, band_v, tri_v,
    s1_send, s1_recv, s2_send, s2_recv, s3_send, s3_recv, pre_v, bsum_v,
    resid_v, stat_v, ostat_v,
    load_sem, param_sem,
    xs_sem, xr_sem, ws_sem, wr_sem, ps_sem, pr_sem, rs_sem, rr_sem, ss_sem, sr_sem,
    hs_sem, hr_sem, m1s_sem, m1r_sem, m2s_sem, m2r_sem, m3s_sem, m3r_sem,
):
    z = lax.axis_index("sp_0")
    x = lax.axis_index("sp_1")
    tp = lax.axis_index("tp")
    sp = z * NX + x
    other = 1 - tp
    n_sp = nz * NX
    after = lax.rem(sp + 1, n_sp)
    prior = lax.rem(sp + n_sp - 1, n_sp)
    partner = {"tp": other}
    x_peers = [{"sp_1": lax.rem(x + d, NX)} for d in range(1, NX)]
    z_peers = [{"sp_0": lax.rem(z + d, nz)} for d in range(1, nz)]
    next_dev = {"sp_0": after // NX, "sp_1": lax.rem(after, NX)}
    prev_dev = {"sp_0": prior // NX, "sp_1": lax.rem(prior, NX)}

    barrier = pltpu.get_barrier_semaphore()
    greeted = [partner] + x_peers + z_peers + [next_dev, prev_dev]
    for dev in greeted:
        pl.semaphore_signal(barrier, inc=1, device_id=dev, device_id_type=MESH)

    own_half = pl.ds(pl.multiple_of(tp * H, H), H)
    oth_half = pl.ds(pl.multiple_of(other * H, H), H)

    def tile(c):
        return pl.ds(c * R, R)

    loads = [
        pltpu.make_async_copy(stream.at[tile(c), :], x_v.at[tile(c), pl.ds(0, H)], load_sem.at[c])
        for c in range(NT)
    ]
    first, second = {}, {}
    for k, (src, dst) in enumerate(((wf, wf_v), (wv, wv_v), (wp, wp_v), (wq, wq_v), (wg, wg_v))):
        first[k] = pltpu.make_async_copy(
            src.at[own_half, :], dst.at[pl.ds(0, H), :], load_sem.at[NT + 2 * k]
        )
        second[k] = pltpu.make_async_copy(
            src.at[oth_half, :], dst.at[pl.ds(H, H), :], load_sem.at[NT + 2 * k + 1]
        )
    params = [
        pltpu.make_async_copy(src, dst, param_sem.at[k])
        for k, (src, dst) in enumerate(
            (
                (lbound, lb_v), (edecay, ed_v), (pmix, pmix_v), (pscale, pscale_v),
                (rgain, rgain_v), (ngain, ngain_v), (nbias, nbias_v),
            )
        )
    ]
    out_loads = [
        pltpu.make_async_copy(
            src.at[:, own_half], wo_v.at[pl.ds(2 * k * C, C), :], load_sem.at[NT + 10 + k]
        )
        for k, src in enumerate((wop, wor))
    ]
    loads[0].start()
    first[0].start()
    for c in range(1, NT):
        loads[c].start()
    first[1].start()
    first[2].start()
    first[3].start()
    for k in range(7):
        params[k].start()
    second[0].start()
    second[1].start()
    second[2].start()
    second[3].start()
    first[4].start()
    second[4].start()
    for c in out_loads:
        c.start()

    row = lax.broadcasted_iota(jnp.int32, (B, B), 0)
    col = lax.broadcasted_iota(jnp.int32, (B, B), 1)
    lower = row >= col
    ones = jnp.where(lower, 1.0, 0.0).astype(BF16)
    tri_v[:, 0:B] = ones
    tri_v[:, B : 2 * B] = ones
    brow = lax.broadcasted_iota(jnp.int32, (B, 2 * B), 0)
    lag = brow + B - lax.broadcasted_iota(jnp.int32, (B, 2 * B), 1)
    for g in range(2):
        width = jnp.left_shift(2, 2 * tp + g)
        band_v[g] = jnp.where((lag >= 0) & (lag < width), 1.0, 0.0).astype(BF16)
    cur_v[...] = jnp.zeros_like(cur_v)
    offcur_v[...] = jnp.zeros_like(offcur_v)
    pooled_v[pl.ds(0, B), :] = jnp.zeros((B, C), BF16)

    first[0].wait()
    for c in range(NT):
        loads[c].wait()
        f_v[tile(c), :] = dot(x_v[tile(c), 0:H], wf_v[0:H, :])

    first[1].wait()
    for c in range(NT):
        resid_v[tile(c), 0:C] = dot(x_v[tile(c), 0:H], wv_v[0:H, :])
    pl.semaphore_wait(barrier, len(greeted))

    def send(src, dst, s_sem, r_sem, dev):
        return pltpu.make_async_remote_copy(
            src_ref=src, dst_ref=dst, send_sem=s_sem, recv_sem=r_sem, device_id=dev, device_id_type=MESH
        )

    x_sends = [
        send(
            x_v.at[tile(c), pl.ds(0, H)], x_v.at[tile(c), pl.ds(H, H)],
            xs_sem.at[c], xr_sem.at[c], partner,
        )
        for c in range(NT)
    ]
    for c in x_sends:
        c.start()
    w_sends = [
        send(
            src.at[:, oth_half], wo_v.at[pl.ds((2 * k + 1) * C, C), :], ws_sem.at[k], wr_sem.at[k], partner
        )
        for k, src in enumerate((wop, wor))
    ]

    first[2].wait()
    for c in range(NT):
        resid_v[tile(c), C : 2 * C] = dot(x_v[tile(c), 0:H], wp_v[0:H, :])
    first[3].wait()
    for c in range(NT):
        gate_v[tile(c), :] = dot(x_v[tile(c), 0:H], wq_v[0:H, :])
    params[0].wait()
    params[1].wait()
    for b in range(NB):
        edc_v[pl.ds(b * B, B), :] = jnp.transpose(ed_v[:, b * B : (b + 1) * B] * LOG2E)

    def forget_dots(c):
        f_v[tile(c), :] = f_v[tile(c), :] + dot(x_v[tile(c), H : 2 * H], wf_v[H : 2 * H, :])
        v_v[tile(c), :] = (
            resid_v[tile(c), 0:C] + dot(x_v[tile(c), H : 2 * H], wv_v[H : 2 * H, :])
        ).astype(BF16)

    def forget_block(b):
        rows = pl.ds(b * B, B)
        ed = edc_v[rows, :]
        off = offcur_v[...]
        off_v[b] = off
        for p in range(NH // 2):
            cols = slice(2 * p * DK, 2 * (p + 1) * DK)
            half_gap = 0.5 - 0.5 * lb_v[:, cols]
            f = f_v[rows, cols].astype(BF16).astype(F32)
            w_in = half_gap - half_gap * jnp.tanh(0.5 * f)
            keep = jnp.log(1.0 - w_in) * LOG2E
            keep = jnp.concatenate(
                [keep[:, k * DK : (k + 1) * DK] + ed[:, 2 * p + k : 2 * p + k + 1] for k in range(2)], axis=1
            )
            hi = keep.astype(BF16)
            lo = (keep - hi.astype(F32)).astype(BF16)
            total = dot(tri_v[...], jnp.concatenate([hi, lo], axis=0))
            end = total[B - 1 : B, :]
            explog_v[rows, cols] = jnp.exp2(total)
            down_v[rows, cols] = (w_in * jnp.exp2(-total)).astype(BF16)
            inw = (w_in * jnp.exp2(end - total)).astype(BF16)
            kept = jnp.exp2(end)
            offcur_v[:, cols] = off[:, cols] + end
            for k in range(2):
                h = 2 * p + k
                hs = slice(k * DK, (k + 1) * DK)
                st = cur_v[h]
                st_v[b, h] = st
                cur_v[h] = kept[:, hs] * st + dot_tn(v_v[rows, h * DK : (h + 1) * DK], inw[:, hs])

    second[0].wait()
    second[1].wait()
    x_sends[0].wait_recv()
    forget_dots(0)
    for c in range(NT):
        if c + 1 < NT:
            x_sends[c + 1].wait_recv()
            forget_dots(c + 1)
        for s in range(R // B):
            forget_block(c * (R // B) + s)

    for h in range(NH):
        s1_send[h, pl.ds(0, DK), :] = cur_v[h].astype(BF16)
        s1_send[h, pl.ds(DK, 16), :] = split_rows(offcur_v[0:1, h * DK : (h + 1) * DK])

    def msg1(d):
        to = lax.rem(x + d, NX)
        return send(s1_send.at[to], s1_recv.at[x], m1s_sem.at[d - 1], m1r_sem.at[x], {"sp_1": to})

    def arrival1(d):
        frm = lax.rem(x + d, NX)
        return send(s1_send.at[frm], s1_recv.at[frm], m1s_sem.at[d - 1], m1r_sem.at[frm], {"sp_1": frm})

    for d in range(1, NX):
        msg1(d).start()
    for c in w_sends:
        c.start()

    second[2].wait()
    for c in range(NT):
        pooled_v[pl.ds(c * R + B, R), :] = (
            resid_v[tile(c), C : 2 * C] + dot(x_v[tile(c), H : 2 * H], wp_v[H : 2 * H, :])
        ).astype(BF16)

    halo = send(pooled_v.at[pl.ds(T + B - 16, 16), :], halo_v, hs_sem, hr_sem, next_dev)
    halo.start()

    second[3].wait()

    def query_dots(c):
        q = gate_v[tile(c), :] + dot(x_v[tile(c), H : 2 * H], wq_v[H : 2 * H, :])
        q = q.astype(BF16).astype(F32)
        up = (silu(q) * explog_v[tile(c), :]).astype(BF16)
        for s in range(R // B):
            rows = pl.ds(c * R + s * B, B)
            for h in range(NH):
                hs = slice(h * DK, (h + 1) * DK)
                u = up[s * B : (s + 1) * B, hs]
                sc = dot_nt(u, down_v[rows, hs])
                sq_v[rows, 2 * h * DK : (2 * h + 1) * DK] = jnp.where(lower, sc, 0.0).astype(BF16)
                sq_v[rows, (2 * h + 1) * DK : (2 * h + 2) * DK] = u

    for c in range(NT):
        query_dots(c)

    s1_recv[x] = s1_send[x]
    for d in range(1, NX):
        arrival1(d).wait_recv()
    run = jnp.zeros((DK, DK), F32)
    logs = jnp.zeros((1, DK), F32)
    for k in range(NX):
        pre_v[k] = run
        bsum_v[k] = jnp.broadcast_to(logs, (8, DK))
        a_k = joined_rows(s1_recv[k, pl.ds(DK, 16), :])
        run = jnp.exp2(a_k) * run + s1_recv[k, pl.ds(0, DK), :].astype(F32)
        logs = logs + a_k
    s2_send[pl.ds(0, DK), :] = run.astype(BF16)
    s2_send[pl.ds(DK, 16), :] = split_rows(logs)

    def msg2(d):
        to = lax.rem(z + d, nz)
        return send(s2_send, s2_recv.at[z], m2s_sem.at[d - 1], m2r_sem.at[z], {"sp_0": to})

    def arrival2(d):
        frm = lax.rem(z + d, nz)
        return send(s2_send, s2_recv.at[frm], m2s_sem.at[d - 1], m2r_sem.at[frm], {"sp_0": frm})

    for d in range(1, nz):
        msg2(d).start()

    first[4].wait()
    second[4].wait()
    for k in range(2, 7):
        params[k].wait()

    def gate_dots(c):
        g = dot(x_v[tile(c), :], wg_v[...]).astype(BF16).astype(F32)
        gain = jnp.concatenate([rgain_v[...]] * NH, axis=1)
        gate_v[tile(c), :] = silu(g) * gain

    for c in range(NT):
        gate_dots(c)

    s2_recv[z] = s2_send[...]
    for d in range(1, nz):
        arrival2(d).wait_recv()
    run = jnp.zeros((DK, DK), F32)
    for k in range(nz - 1):
        b_k = joined_rows(s2_recv[k, pl.ds(DK, 16), :])
        new = jnp.exp2(b_k) * run + s2_recv[k, pl.ds(0, DK), :].astype(F32)
        run = jnp.where(k < z, new, run)
    for k in range(NX):
        s3_send[k] = (jnp.exp2(bsum_v[k][0:1, :]) * run + pre_v[k]).astype(BF16)

    def msg3(d):
        to = lax.rem(x + d, NX)
        return send(s3_send.at[to], s3_recv.at[x], m3s_sem.at[d - 1], m3r_sem.at[x], {"sp_1": to})

    def arrival3(d):
        frm = lax.rem(x + d, NX)
        return send(s3_send.at[frm], s3_recv.at[frm], m3s_sem.at[d - 1], m3r_sem.at[frm], {"sp_1": frm})

    for d in range(1, NX):
        msg3(d).start()

    halo.wait_recv()
    pooled_v[pl.ds(B - 16, 16), :] = jnp.where(sp > 0, halo_v[...], jnp.zeros_like(halo_v))

    pool_sends = [
        send(a_v.at[tile(c), pl.ds(0, C)], a_v.at[tile(c), pl.ds(C, C)], ps_sem.at[c], pr_sem.at[c], partner)
        for c in range(NT)
    ]

    def pooling(b):
        position = sp * T + b * B + lax.broadcasted_iota(jnp.int32, (B, 1), 0) + 1
        for g in range(2):
            cols = slice(g * 256, (g + 1) * 256)
            total = dot(band_v[g], pooled_v[pl.ds(b * B, 2 * B), cols])
            here = pooled_v[pl.ds((b + 1) * B, B), cols].astype(F32)
            width = jnp.left_shift(2, 2 * tp + g)
            if b == 0:
                diff = total / jnp.minimum(position, width).astype(F32) - here
            else:
                diff = total * (1.0 / width.astype(F32)) - here
            mixed = dot(diff.astype(BF16), pmix_v[g]) * pscale_v[:, cols]
            a_v[pl.ds(b * B, B), cols] = mixed.astype(BF16)

    for c in range(NT):
        for s in range(R // B):
            pooling(c * (R // B) + s)
        pool_sends[c].start()

    for c in out_loads:
        c.wait()
    for c in w_sends:
        c.wait_recv()
    for c in range(NT):
        pool_sends[c].wait_recv()
        resid_v[tile(c), :] = ALPHA * x_v[tile(c), 0:H].astype(F32) + dot(
            a_v[tile(c), 0 : 2 * C], wo_v[0 : 2 * C, :]
        )

    s3_recv[x] = s3_send[x]
    for d in range(1, NX):
        arrival3(d).wait_recv()

    rec_sends = [
        send(
            a_v.at[tile(c), pl.ds(2 * C, C)], a_v.at[tile(c), pl.ds(3 * C, C)],
            rs_sem.at[c], rr_sem.at[c], partner,
        )
        for c in range(NT)
    ]
    stat_sends = [
        send(stat_v.at[tile(c), :], ostat_v.at[tile(c), :], ss_sem.at[c], sr_sem.at[c], partner)
        for c in range(NT)
    ]

    def recur(b):
        rows = pl.ds(b * B, B)
        far = jnp.exp2(off_v[b])
        for h in range(NH):
            hs = slice(h * DK, (h + 1) * DK)
            state = st_v[b, h] + far[:, hs] * s3_recv[h].astype(F32)
            raw = dot(sq_v[rows, 2 * h * DK : (2 * h + 1) * DK], v_v[rows, hs])
            raw = raw + dot_nt(sq_v[rows, (2 * h + 1) * DK : (2 * h + 2) * DK], state.astype(BF16))
            power = jnp.mean(raw * raw, axis=1, keepdims=True)
            normed = raw * lax.rsqrt(power + EPS_RMS) * gate_v[rows, hs]
            a_v[rows, 2 * C + h * DK : 2 * C + (h + 1) * DK] = normed.astype(BF16)

    def project(c):
        resid = resid_v[tile(c), :] + dot(a_v[tile(c), 2 * C : 4 * C], wo_v[2 * C : 4 * C, :])
        resid_v[tile(c), :] = resid
        mean = jnp.sum(resid, axis=1, keepdims=True) * (1.0 / H)
        dev = resid - mean
        m2 = jnp.sum(dev * dev, axis=1, keepdims=True)
        lane = lax.broadcasted_iota(jnp.int32, (R, DK), 1)
        stat_v[tile(c), :] = jnp.where(lane == 0, mean, m2)

    def norm(c):
        mine = stat_v[tile(c), :]
        theirs = ostat_v[tile(c), :]
        gap = mine[:, 0:1] - theirs[:, 0:1]
        mean = 0.5 * (mine[:, 0:1] + theirs[:, 0:1])
        var = (mine[:, 1:2] + theirs[:, 1:2] + gap * gap * (0.5 * H)) * (1.0 / (2 * H))
        scale = lax.rsqrt(var + EPS_NORM)
        out[tile(c), :] = (
            (resid_v[tile(c), :] - mean) * scale * ngain_v[...] + nbias_v[...]
        ).astype(BF16)

    for j in range(-2, NT + 2):
        if 0 <= j < NT:
            rec_sends[j].wait_recv()
        if j >= 2:
            stat_sends[j - 2].wait_recv()
        if j + 2 < NT:
            for s in range(R // B):
                recur((j + 2) * (R // B) + s)
        if 0 <= j < NT:
            project(j)
        if j >= 2:
            norm(j - 2)
        if j + 2 < NT:
            rec_sends[j + 2].start()
        if 0 <= j < NT:
            stat_sends[j].start()

    for c in range(NT):
        x_sends[c].wait_send()
        pool_sends[c].wait_send()
        rec_sends[c].wait_send()
        stat_sends[c].wait_send()
    for c in w_sends:
        c.wait_send()
    halo.wait_send()
    for d in range(1, NX):
        msg1(d).wait_send()
        msg3(d).wait_send()
    for d in range(1, nz):
        msg2(d).wait_send()


def layer(nz, *args):
    (stream, wp, wq, wf, wv, wg, pmix, pscale, lb, ed, rgain, wop, wor, ngain, nbias) = args
    sem = pltpu.SemaphoreType.DMA
    scratch = [
        pltpu.VMEM((T, 2 * H), BF16),
        *[pltpu.VMEM((2 * H, C), BF16)] * 5,
        pltpu.VMEM((4 * C, H), BF16),
        pltpu.VMEM((2, 256, 256), BF16),
        pltpu.VMEM((1, C), F32),
        pltpu.VMEM((1, C), F32),
        pltpu.VMEM((NH, T), F32),
        pltpu.VMEM((T, NH), F32),
        pltpu.VMEM((1, DK), F32),
        pltpu.VMEM((1, H), F32),
        pltpu.VMEM((1, H), F32),
        pltpu.VMEM((T, C), F32),
        pltpu.VMEM((T, C), BF16),
        pltpu.VMEM((T, C), F32),
        pltpu.VMEM((T, C), BF16),
        pltpu.VMEM((T + B, C), BF16),
        pltpu.VMEM((16, C), BF16),
        pltpu.VMEM((T, 2 * C), BF16),
        pltpu.VMEM((T, C), F32),
        pltpu.VMEM((T, 4 * C), BF16),
        pltpu.VMEM((NB, NH, DK, DK), F32),
        pltpu.VMEM((NH, DK, DK), F32),
        pltpu.VMEM((NB, 1, C), F32),
        pltpu.VMEM((1, C), F32),
        pltpu.VMEM((2, B, 2 * B), BF16),
        pltpu.VMEM((B, 2 * B), BF16),
        pltpu.VMEM((NH, MSG, DK), BF16),
        pltpu.VMEM((NX, MSG, DK), BF16),
        pltpu.VMEM((MSG, DK), BF16),
        pltpu.VMEM((nz, MSG, DK), BF16),
        pltpu.VMEM((NX, DK, DK), BF16),
        pltpu.VMEM((NX, DK, DK), BF16),
        pltpu.VMEM((NX, DK, DK), F32),
        pltpu.VMEM((NX, 8, DK), F32),
        pltpu.VMEM((T, H), F32),
        pltpu.VMEM((T, DK), F32),
        pltpu.VMEM((T, DK), F32),
        sem((NT + 12,)), sem((7,)),
        sem((NT,)), sem((NT,)), sem((2,)), sem((2,)), sem((NT,)), sem((NT,)),
        sem((NT,)), sem((NT,)), sem((NT,)), sem((NT,)),
        sem, sem,
        sem((NX - 1,)), sem((NX,)), sem((nz - 1,)), sem((nz,)), sem((NX - 1,)), sem((NX,)),
    ]
    operands = (
        stream[0], wp, wq, wf, wv, wg, pmix,
        pscale.reshape(1, C), lb.reshape(1, C), ed.T, rgain.reshape(1, DK),
        wop, wor, ngain.reshape(1, H), nbias.reshape(1, H),
    )
    result = pl.pallas_call(
        functools.partial(kernel, nz),
        out_shape=pltpu.VMEM((T, H), BF16),
        in_specs=[pl.BlockSpec(memory_space=pltpu.HBM)] * 15,
        out_specs=pl.BlockSpec(memory_space=pltpu.VMEM),
        scratch_shapes=scratch,
        compiler_params=pltpu.CompilerParams(
            collective_id=0, has_side_effects=True, vmem_limit_bytes=58_000_000
        ),
    )(*[pltpu.with_memory_space_constraint(a, pltpu.HBM) for a in operands])
    return result[None]


def solution(mesh):
    devices = mesh.devices
    nz = devices.shape[0] // NX
    torus = Mesh(
        devices.reshape(nz, NX, mesh.shape["fs"], mesh.shape["tp"]), ("sp_0", "sp_1", "fs", "tp")
    )
    sp = ("sp_0", "sp_1")
    cols = P(None, "tp")
    return jax.shard_map(
        functools.partial(layer, nz),
        mesh=torus,
        in_specs=(
            P("fs", sp, "tp"), cols, cols, cols, cols, cols,
            P("tp", None, None), P("tp"), P("tp"), P(sp, "tp"), P(),
            P("tp", None), P("tp", None), P("tp"), P("tp"),
        ),
        out_specs=P("fs", sp, "tp"),
        check_vma=False,
    )
```

time: 53.5 us -> 40.1 us (0.75)
  Pallas kernels: 48.5 us -> 38.7 us
  local copies, waits for them, and re-layouts: 4.82 us -> 1.32 us
    pallas_call x1, Pallas kernels: 48.5 us -> 38.7 us  [layer(): pl.pallas_call(functools.partial(kernel, nz), out_shape=pltpu.VMEM((T, H)...]
    unnamed x2 -> x1, local copies, waits for them, and re-layouts: 4.82 us -> 1.32 us
where the time goes in v2:
time: 40.1 us; the launch traced here: 40 us
  Pallas kernels  38.7 us (97%)
  local copies, waits for them, and re-layouts  1.32 us (3%)
    pallas_call x1, Pallas kernels, layer(): pl.pallas_call(functools.partial(kernel, nz), out_shape=pltpu.VMEM((T, H)...  38.7 us
    unnamed x1, local copies, waits for them, and re-layouts  1.32 us

profile of v2, /device:TPU:1, one launch (start us, length us, event | category | flops | bytes accessed | tf_op | source)
XLA Modules:
  0.0 40.0 jit_solution(13936603260509341377)
XLA Ops:
  0.0 38.7 %shard_map.145 = bf16[1024,1024]{1,0:T(8,128)(2,1)S(1)} custom-call(bf16[1024,1024]{1,0:T(8,128)(2,1)} %bitcast.9, bf16[2048,512]{1,0:T(8,128)(2,1)} %wp.1, bf16[2048,512]{1,0:T(8,128)(2,1)} %wq.1, bf16[2048,512]{1,0:T(8,128)(2,1)} %wf.1, bf16[2048,512]{1,0:T(8,128)(2,1)} %wv.1, bf16[2048,512]{1,0:T(8,128)(2,1)} %wg.1, bf16[2,256,256]{2,1,0:T(8,128)(2,1)} %pmix.1, ...), custom_call_target="tpu_custom_call" | custom-call | tf_op jit(solution)/shard_map/pallas_call | solution.py:529
  38.7 1.3 %copy.17 = bf16[1,1024,1024]{2,1,0:T(8,128)(2,1)} copy(bf16[1,1024,1024]{2,1,0:T(8,128)(2,1)S(1)} %bitcast.8) | data formatting | bytes 4194304

commit v3 on v2

--- a/solution.py
+++ b/solution.py
@@ -73,7 +73,7 @@
     pmix_v, pscale_v, lb_v, ed_v, edc_v, rgain_v, ngain_v, nbias_v,
     f_v, v_v, explog_v, down_v, pooled_v, halo_v, sq_v, gate_v, a_v,
     st_v, cur_v, off_v, offcur_v, band_v, tri_v,
-    s1_send, s1_recv, s2_send, s2_recv, s3_send, s3_recv, pre_v, bsum_v,
+    s1_send, s1_recv, s2_send, s2_recv, s3_send, s3_recv, pre_v, bsum_v, run_v,
     resid_v, stat_v, ostat_v,
     load_sem, param_sem,
     xs_sem, xr_sem, ws_sem, wr_sem, ps_sem, pr_sem, rs_sem, rr_sem, ss_sem, sr_sem,
@@ -87,6 +87,7 @@
     n_sp = nz * NX
     after = lax.rem(sp + 1, n_sp)
     prior = lax.rem(sp + n_sp - 1, n_sp)
+    is_first, is_last = sp == 0, sp == n_sp - 1
     partner = {"tp": other}
     x_peers = [{"sp_1": lax.rem(x + d, NX)} for d in range(1, NX)]
     z_peers = [{"sp_0": lax.rem(z + d, nz)} for d in range(1, nz)]
@@ -94,9 +95,18 @@
     prev_dev = {"sp_0": prior // NX, "sp_1": lax.rem(prior, NX)}
 
     barrier = pltpu.get_barrier_semaphore()
-    greeted = [partner] + x_peers + z_peers + [next_dev, prev_dev]
+    greeted = [partner] + x_peers + z_peers
     for dev in greeted:
         pl.semaphore_signal(barrier, inc=1, device_id=dev, device_id_type=MESH)
+
+    @pl.when(jnp.logical_not(is_last))
+    def _():
+        pl.semaphore_signal(barrier, inc=1, device_id=next_dev, device_id_type=MESH)
+
+    @pl.when(jnp.logical_not(is_first))
+    def _():
+        pl.semaphore_signal(barrier, inc=1, device_id=prev_dev, device_id_type=MESH)
+
 
     own_half = pl.ds(pl.multiple_of(tp * H, H), H)
     oth_half = pl.ds(pl.multiple_of(other * H, H), H)
@@ -172,7 +182,7 @@
     first[1].wait()
     for c in range(NT):
         resid_v[tile(c), 0:C] = dot(x_v[tile(c), 0:H], wv_v[0:H, :])
-    pl.semaphore_wait(barrier, len(greeted))
+    pl.semaphore_wait(barrier, len(greeted) + jnp.minimum(sp, 1) + jnp.minimum(n_sp - 1 - sp, 1))
 
     def send(src, dst, s_sem, r_sem, dev):
         return pltpu.make_async_remote_copy(
@@ -277,7 +287,10 @@
         ).astype(BF16)
 
     halo = send(pooled_v.at[pl.ds(T + B - 16, 16), :], halo_v, hs_sem, hr_sem, next_dev)
-    halo.start()
+
+    @pl.when(jnp.logical_not(is_last))
+    def _():
+        halo.start()
 
     second[3].wait()
 
@@ -311,16 +324,14 @@
     s2_send[pl.ds(0, DK), :] = run.astype(BF16)
     s2_send[pl.ds(DK, 16), :] = split_rows(logs)
 
-    def msg2(d):
-        to = lax.rem(z + d, nz)
-        return send(s2_send, s2_recv.at[z], m2s_sem.at[d - 1], m2r_sem.at[z], {"sp_0": to})
-
-    def arrival2(d):
-        frm = lax.rem(z + d, nz)
-        return send(s2_send, s2_recv.at[frm], m2s_sem.at[d - 1], m2r_sem.at[frm], {"sp_0": frm})
-
-    for d in range(1, nz):
-        msg2(d).start()
+    def msg2(k):
+        return send(s2_send, s2_recv.at[z], m2s_sem.at[k], m2r_sem.at[z], {"sp_0": k})
+
+    for k in range(1, nz):
+
+        @pl.when(k > z)
+        def _():
+            msg2(k).start()
 
     first[4].wait()
     second[4].wait()
@@ -335,14 +346,16 @@
     for c in range(NT):
         gate_dots(c)
 
-    s2_recv[z] = s2_send[...]
-    for d in range(1, nz):
-        arrival2(d).wait_recv()
-    run = jnp.zeros((DK, DK), F32)
+    run_v[...] = jnp.zeros_like(run_v)
     for k in range(nz - 1):
-        b_k = joined_rows(s2_recv[k, pl.ds(DK, 16), :])
-        new = jnp.exp2(b_k) * run + s2_recv[k, pl.ds(0, DK), :].astype(F32)
-        run = jnp.where(k < z, new, run)
+
+        @pl.when(k < z)
+        def _():
+            send(s2_send, s2_recv.at[k], m2s_sem.at[k], m2r_sem.at[k], {"sp_0": k}).wait_recv()
+            b_k = joined_rows(s2_recv[k, pl.ds(DK, 16), :])
+            run_v[...] = jnp.exp2(b_k) * run_v[...] + s2_recv[k, pl.ds(0, DK), :].astype(F32)
+
+    run = run_v[...]
     for k in range(NX):
         s3_send[k] = (jnp.exp2(bsum_v[k][0:1, :]) * run + pre_v[k]).astype(BF16)
 
@@ -357,8 +370,10 @@
     for d in range(1, NX):
         msg3(d).start()
 
-    halo.wait_recv()
-    pooled_v[pl.ds(B - 16, 16), :] = jnp.where(sp > 0, halo_v[...], jnp.zeros_like(halo_v))
+    @pl.when(jnp.logical_not(is_first))
+    def _():
+        halo.wait_recv()
+        pooled_v[pl.ds(B - 16, 16), :] = halo_v[...]
 
     pool_sends = [
         send(a_v.at[tile(c), pl.ds(0, C)], a_v.at[tile(c), pl.ds(C, C)], ps_sem.at[c], pr_sem.at[c], partner)
@@ -388,11 +403,14 @@
         c.wait()
     for c in w_sends:
         c.wait_recv()
-    for c in range(NT):
+    def pool_project(c):
         pool_sends[c].wait_recv()
         resid_v[tile(c), :] = ALPHA * x_v[tile(c), 0:H].astype(F32) + dot(
             a_v[tile(c), 0 : 2 * C], wo_v[0 : 2 * C, :]
         )
+
+    for c in range(NT - 1):
+        pool_project(c)
 
     s3_recv[x] = s3_send[x]
     for d in range(1, NX):
@@ -442,22 +460,26 @@
             (resid_v[tile(c), :] - mean) * scale * ngain_v[...] + nbias_v[...]
         ).astype(BF16)
 
-    for j in range(-2, NT + 2):
-        if 0 <= j < NT:
-            rec_sends[j].wait_recv()
-        if j >= 2:
-            stat_sends[j - 2].wait_recv()
-        if j + 2 < NT:
-            for s in range(R // B):
-                recur((j + 2) * (R // B) + s)
-        if 0 <= j < NT:
-            project(j)
-        if j >= 2:
-            norm(j - 2)
-        if j + 2 < NT:
-            rec_sends[j + 2].start()
-        if 0 <= j < NT:
-            stat_sends[j].start()
+    def recur_tile(c):
+        for k in range(R // B):
+            recur(c * (R // B) + k)
+        rec_sends[c].start()
+
+    recur_tile(0)
+    pool_project(NT - 1)
+    recur_tile(1)
+    for c in range(NT):
+        rec_sends[c].wait_recv()
+        if c + 2 < NT:
+            for k in range(R // B):
+                recur((c + 2) * (R // B) + k)
+        project(c)
+        if c + 2 < NT:
+            rec_sends[c + 2].start()
+        stat_sends[c].start()
+    for c in range(NT):
+        stat_sends[c].wait_recv()
+        norm(c)
 
     for c in range(NT):
         x_sends[c].wait_send()
@@ -466,12 +488,19 @@
         stat_sends[c].wait_send()
     for c in w_sends:
         c.wait_send()
-    halo.wait_send()
+
+    @pl.when(jnp.logical_not(is_last))
+    def _():
+        halo.wait_send()
+
     for d in range(1, NX):
         msg1(d).wait_send()
         msg3(d).wait_send()
-    for d in range(1, nz):
-        msg2(d).wait_send()
+    for k in range(1, nz):
+
+        @pl.when(k > z)
+        def _():
+            msg2(k).wait_send()
 
 
 def layer(nz, *args):
@@ -512,6 +541,7 @@
         pltpu.VMEM((NX, DK, DK), BF16),
         pltpu.VMEM((NX, DK, DK), F32),
         pltpu.VMEM((NX, 8, DK), F32),
+        pltpu.VMEM((DK, DK), F32),
         pltpu.VMEM((T, H), F32),
         pltpu.VMEM((T, DK), F32),
         pltpu.VMEM((T, DK), F32),
@@ -519,7 +549,7 @@
         sem((NT,)), sem((NT,)), sem((2,)), sem((2,)), sem((NT,)), sem((NT,)),
         sem((NT,)), sem((NT,)), sem((NT,)), sem((NT,)),
         sem, sem,
-        sem((NX - 1,)), sem((NX,)), sem((nz - 1,)), sem((nz,)), sem((NX - 1,)), sem((NX,)),
+        sem((NX - 1,)), sem((NX,)), sem((nz,)), sem((nz,)), sem((NX - 1,)), sem((NX,)),
     ]
     operands = (
         stream[0], wp, wq, wf, wv, wg, pmix,

time: 40.1 us -> 35.1 us (0.88)
  Pallas kernels: 38.7 us -> 33.7 us
    pallas_call x1, Pallas kernels: 38.7 us -> 33.7 us  [layer(): pl.pallas_call(functools.partial(kernel, nz), out_shape=pltpu.VMEM((T, H)...]
where the time goes in v3:
time: 35.1 us; the launch traced here: 35 us
  Pallas kernels  33.7 us (96%)
  local copies, waits for them, and re-layouts  1.32 us (4%)
    pallas_call x1, Pallas kernels, layer(): pl.pallas_call(functools.partial(kernel, nz), out_shape=pltpu.VMEM((T, H)...  33.7 us
    unnamed x1, local copies, waits for them, and re-layouts  1.32 us

profile of v3, /device:TPU:1, one launch (start us, length us, event | category | flops | bytes accessed | tf_op | source)
XLA Modules:
  0.0 35.0 jit_solution(16117595587203762928)
XLA Ops:
  0.0 33.7 %shard_map.145 = bf16[1024,1024]{1,0:T(8,128)(2,1)S(1)} custom-call(bf16[1024,1024]{1,0:T(8,128)(2,1)} %bitcast.9, bf16[2048,512]{1,0:T(8,128)(2,1)} %wp.1, bf16[2048,512]{1,0:T(8,128)(2,1)} %wq.1, bf16[2048,512]{1,0:T(8,128)(2,1)} %wf.1, bf16[2048,512]{1,0:T(8,128)(2,1)} %wv.1, bf16[2048,512]{1,0:T(8,128)(2,1)} %wg.1, bf16[2,256,256]{2,1,0:T(8,128)(2,1)} %pmix.1, ...), custom_call_target="tpu_custom_call" | custom-call | tf_op jit(solution)/shard_map/pallas_call | solution.py:559
  33.7 1.3 %copy.17 = bf16[1,1024,1024]{2,1,0:T(8,128)(2,1)} copy(bf16[1,1024,1024]{2,1,0:T(8,128)(2,1)S(1)} %bitcast.8) | data formatting | bytes 4194304

commit v4 on v3

--- a/solution.py
+++ b/solution.py
@@ -27,6 +27,8 @@
 NB = T // B
 R = 256
 NT = T // R
+RB = 512
+NB_BIG = T // RB
 NX = 4
 MSG = DK + 16
 
@@ -114,6 +116,9 @@
     def tile(c):
         return pl.ds(c * R, R)
 
+    def big(c):
+        return pl.ds(c * RB, RB)
+
     loads = [
         pltpu.make_async_copy(stream.at[tile(c), :], x_v.at[tile(c), pl.ds(0, H)], load_sem.at[c])
         for c in range(NT)
@@ -141,23 +146,23 @@
         )
         for k, src in enumerate((wop, wor))
     ]
-    loads[0].start()
-    first[0].start()
+    def start_x(c):
+        for k in range(2):
+            rows = pl.ds(c * R + k * (R // 2), R // 2)
+            pltpu.make_async_copy(stream.at[rows, :], x_v.at[rows, pl.ds(0, H)], load_sem.at[c]).start()
+
+    start_x(0)
+    for k in range(4):
+        pltpu.make_async_copy(
+            wf.at[pl.ds(pl.multiple_of(tp * H + k * 256, 256), 256), :],
+            wf_v.at[pl.ds(k * 256, 256), :],
+            load_sem.at[NT],
+        ).start()
     for c in range(1, NT):
-        loads[c].start()
+        start_x(c)
     first[1].start()
-    first[2].start()
-    first[3].start()
     for k in range(7):
         params[k].start()
-    second[0].start()
-    second[1].start()
-    second[2].start()
-    second[3].start()
-    first[4].start()
-    second[4].start()
-    for c in out_loads:
-        c.start()
 
     row = lax.broadcasted_iota(jnp.int32, (B, B), 0)
     col = lax.broadcasted_iota(jnp.int32, (B, B), 1)
@@ -179,9 +184,14 @@
         loads[c].wait()
         f_v[tile(c), :] = dot(x_v[tile(c), 0:H], wf_v[0:H, :])
 
+    for k in (2, 3):
+        first[k].start()
+    for k in (0, 1, 2, 3):
+        second[k].start()
+
     first[1].wait()
-    for c in range(NT):
-        resid_v[tile(c), 0:C] = dot(x_v[tile(c), 0:H], wv_v[0:H, :])
+    for c in range(NB_BIG):
+        resid_v[big(c), 0:C] = dot(x_v[big(c), 0:H], wv_v[0:H, :])
     pl.semaphore_wait(barrier, len(greeted) + jnp.minimum(sp, 1) + jnp.minimum(n_sp - 1 - sp, 1))
 
     def send(src, dst, s_sem, r_sem, dev):
@@ -206,11 +216,15 @@
     ]
 
     first[2].wait()
-    for c in range(NT):
-        resid_v[tile(c), C : 2 * C] = dot(x_v[tile(c), 0:H], wp_v[0:H, :])
+    for c in range(NB_BIG):
+        resid_v[big(c), C : 2 * C] = dot(x_v[big(c), 0:H], wp_v[0:H, :])
+    first[4].start()
+    second[4].start()
+    for c in out_loads:
+        c.start()
     first[3].wait()
-    for c in range(NT):
-        gate_v[tile(c), :] = dot(x_v[tile(c), 0:H], wq_v[0:H, :])
+    for c in range(NB_BIG):
+        gate_v[big(c), :] = dot(x_v[big(c), 0:H], wq_v[0:H, :])
     params[0].wait()
     params[1].wait()
     for b in range(NB):
@@ -220,6 +234,11 @@
         f_v[tile(c), :] = f_v[tile(c), :] + dot(x_v[tile(c), H : 2 * H], wf_v[H : 2 * H, :])
         v_v[tile(c), :] = (
             resid_v[tile(c), 0:C] + dot(x_v[tile(c), H : 2 * H], wv_v[H : 2 * H, :])
+        ).astype(BF16)
+
+    def pooled_dots(c):
+        pooled_v[pl.ds(c * RB + B, RB), :] = (
+            resid_v[big(c), C : 2 * C] + dot(x_v[big(c), H : 2 * H], wp_v[H : 2 * H, :])
         ).astype(BF16)
 
     def forget_block(b):
@@ -230,8 +249,7 @@
         for p in range(NH // 2):
             cols = slice(2 * p * DK, 2 * (p + 1) * DK)
             half_gap = 0.5 - 0.5 * lb_v[:, cols]
-            f = f_v[rows, cols].astype(BF16).astype(F32)
-            w_in = half_gap - half_gap * jnp.tanh(0.5 * f)
+            w_in = half_gap - half_gap * jnp.tanh(0.5 * f_v[rows, cols])
             keep = jnp.log(1.0 - w_in) * LOG2E
             keep = jnp.concatenate(
                 [keep[:, k * DK : (k + 1) * DK] + ed[:, 2 * p + k : 2 * p + k + 1] for k in range(2)], axis=1
@@ -256,10 +274,13 @@
     second[1].wait()
     x_sends[0].wait_recv()
     forget_dots(0)
+    second[2].wait()
     for c in range(NT):
         if c + 1 < NT:
             x_sends[c + 1].wait_recv()
             forget_dots(c + 1)
+        else:
+            pooled_dots(0)
         for s in range(R // B):
             forget_block(c * (R // B) + s)
 
@@ -275,16 +296,12 @@
         frm = lax.rem(x + d, NX)
         return send(s1_send.at[frm], s1_recv.at[frm], m1s_sem.at[d - 1], m1r_sem.at[frm], {"sp_1": frm})
 
-    for d in range(1, NX):
+    for d in (2, 1, 3):
         msg1(d).start()
     for c in w_sends:
         c.start()
 
-    second[2].wait()
-    for c in range(NT):
-        pooled_v[pl.ds(c * R + B, R), :] = (
-            resid_v[tile(c), C : 2 * C] + dot(x_v[tile(c), H : 2 * H], wp_v[H : 2 * H, :])
-        ).astype(BF16)
+    pooled_dots(1)
 
     halo = send(pooled_v.at[pl.ds(T + B - 16, 16), :], halo_v, hs_sem, hr_sem, next_dev)
 
@@ -296,7 +313,6 @@
 
     def query_dots(c):
         q = gate_v[tile(c), :] + dot(x_v[tile(c), H : 2 * H], wq_v[H : 2 * H, :])
-        q = q.astype(BF16).astype(F32)
         up = (silu(q) * explog_v[tile(c), :]).astype(BF16)
         for s in range(R // B):
             rows = pl.ds(c * R + s * B, B)
@@ -310,28 +326,62 @@
     for c in range(NT):
         query_dots(c)
 
-    s1_recv[x] = s1_send[x]
-    for d in range(1, NX):
-        arrival1(d).wait_recv()
-    run = jnp.zeros((DK, DK), F32)
-    logs = jnp.zeros((1, DK), F32)
-    for k in range(NX):
-        pre_v[k] = run
-        bsum_v[k] = jnp.broadcast_to(logs, (8, DK))
-        a_k = joined_rows(s1_recv[k, pl.ds(DK, 16), :])
-        run = jnp.exp2(a_k) * run + s1_recv[k, pl.ds(0, DK), :].astype(F32)
-        logs = logs + a_k
-    s2_send[pl.ds(0, DK), :] = run.astype(BF16)
-    s2_send[pl.ds(DK, 16), :] = split_rows(logs)
-
     def msg2(k):
         return send(s2_send, s2_recv.at[z], m2s_sem.at[k], m2r_sem.at[z], {"sp_0": k})
 
-    for k in range(1, nz):
-
-        @pl.when(k > z)
+    def msg3(d):
+        to = lax.rem(x + d, NX)
+        return send(s3_send.at[to], s3_recv.at[x], m3s_sem.at[d - 1], m3r_sem.at[x], {"sp_1": to})
+
+    def arrival3(d):
+        frm = lax.rem(x + d, NX)
+        return send(s3_send.at[frm], s3_recv.at[frm], m3s_sem.at[d - 1], m3r_sem.at[frm], {"sp_1": frm})
+
+    def row_prefix():
+        s1_recv[x] = s1_send[x]
+        for d in range(1, NX):
+            arrival1(d).wait_recv()
+        run = jnp.zeros((DK, DK), F32)
+        logs = jnp.zeros((1, DK), F32)
+        for k in range(NX):
+            pre_v[k] = run
+            bsum_v[k] = jnp.broadcast_to(logs, (8, DK))
+            a_k = joined_rows(s1_recv[k, pl.ds(DK, 16), :])
+            run = jnp.exp2(a_k) * run + s1_recv[k, pl.ds(0, DK), :].astype(F32)
+            logs = logs + a_k
+        s2_send[pl.ds(0, DK), :] = run.astype(BF16)
+        s2_send[pl.ds(DK, 16), :] = split_rows(logs)
+
+        for k in range(1, nz):
+
+            @pl.when(k > z)
+            def _():
+                msg2(k).start()
+
+    def column_prefix():
+        run_v[...] = jnp.zeros_like(run_v)
+        for k in range(nz - 1):
+
+            @pl.when(k < z)
+            def _():
+                send(s2_send, s2_recv.at[k], m2s_sem.at[k], m2r_sem.at[k], {"sp_0": k}).wait_recv()
+                b_k = joined_rows(s2_recv[k, pl.ds(DK, 16), :])
+                run_v[...] = jnp.exp2(b_k) * run_v[...] + s2_recv[k, pl.ds(0, DK), :].astype(F32)
+
+        run = run_v[...]
+        for k in range(NX):
+            s3_send[k] = (jnp.exp2(bsum_v[k][0:1, :]) * run + pre_v[k]).astype(BF16)
+
+        for d in (2, 1, 3):
+            msg3(d).start()
+
+    @pl.when(x > 0)
+    def _():
+        row_prefix()
+
+        @pl.when(z == 0)
         def _():
-            msg2(k).start()
+            column_prefix()
 
     first[4].wait()
     second[4].wait()
@@ -339,41 +389,9 @@
         params[k].wait()
 
     def gate_dots(c):
-        g = dot(x_v[tile(c), :], wg_v[...]).astype(BF16).astype(F32)
+        g = dot(x_v[tile(c), :], wg_v[...])
         gain = jnp.concatenate([rgain_v[...]] * NH, axis=1)
         gate_v[tile(c), :] = silu(g) * gain
-
-    for c in range(NT):
-        gate_dots(c)
-
-    run_v[...] = jnp.zeros_like(run_v)
-    for k in range(nz - 1):
-
-        @pl.when(k < z)
-        def _():
-            send(s2_send, s2_recv.at[k], m2s_sem.at[k], m2r_sem.at[k], {"sp_0": k}).wait_recv()
-            b_k = joined_rows(s2_recv[k, pl.ds(DK, 16), :])
-            run_v[...] = jnp.exp2(b_k) * run_v[...] + s2_recv[k, pl.ds(0, DK), :].astype(F32)
-
-    run = run_v[...]
-    for k in range(NX):
-        s3_send[k] = (jnp.exp2(bsum_v[k][0:1, :]) * run + pre_v[k]).astype(BF16)
-
-    def msg3(d):
-        to = lax.rem(x + d, NX)
-        return send(s3_send.at[to], s3_recv.at[x], m3s_sem.at[d - 1], m3r_sem.at[x], {"sp_1": to})
-
-    def arrival3(d):
-        frm = lax.rem(x + d, NX)
-        return send(s3_send.at[frm], s3_recv.at[frm], m3s_sem.at[d - 1], m3r_sem.at[frm], {"sp_1": frm})
-
-    for d in range(1, NX):
-        msg3(d).start()
-
-    @pl.when(jnp.logical_not(is_first))
-    def _():
-        halo.wait_recv()
-        pooled_v[pl.ds(B - 16, 16), :] = halo_v[...]
 
     pool_sends = [
         send(a_v.at[tile(c), pl.ds(0, C)], a_v.at[tile(c), pl.ds(C, C)], ps_sem.at[c], pr_sem.at[c], partner)
@@ -394,22 +412,57 @@
             mixed = dot(diff.astype(BF16), pmix_v[g]) * pscale_v[:, cols]
             a_v[pl.ds(b * B, B), cols] = mixed.astype(BF16)
 
-    for c in range(NT):
-        for s in range(R // B):
-            pooling(c * (R // B) + s)
-        pool_sends[c].start()
+    def pool_tiles(c):
+        for k in range(R // B):
+            pooling(c * (R // B) + k)
+
+    gate_dots(0)
+    gate_dots(1)
+    pool_tiles(1)
+    pool_sends[1].start()
+
+    @pl.when(x == 0)
+    def _():
+        row_prefix()
+
+        @pl.when(z == 0)
+        def _():
+            column_prefix()
+
+    @pl.when((x > 0) & (z > 0))
+    def _():
+        column_prefix()
+
+    gate_dots(2)
+    pool_tiles(2)
+    pool_sends[2].start()
+
+    @pl.when((x == 0) & (z > 0))
+    def _():
+        column_prefix()
+
+    @pl.when(jnp.logical_not(is_first))
+    def _():
+        halo.wait_recv()
+        pooled_v[pl.ds(B - 16, 16), :] = halo_v[...]
+
+    gate_dots(3)
+    pool_tiles(3)
+    pool_tiles(0)
+    pool_sends[3].start()
+    pool_sends[0].start()
 
     for c in out_loads:
         c.wait()
     for c in w_sends:
         c.wait_recv()
     def pool_project(c):
-        pool_sends[c].wait_recv()
         resid_v[tile(c), :] = ALPHA * x_v[tile(c), 0:H].astype(F32) + dot(
             a_v[tile(c), 0 : 2 * C], wo_v[0 : 2 * C, :]
         )
 
-    for c in range(NT - 1):
+    for c in range(1, NT):
+        pool_sends[c].wait_recv()
         pool_project(c)
 
     s3_recv[x] = s3_send[x]
@@ -441,8 +494,12 @@
             a_v[rows, 2 * C + h * DK : 2 * C + (h + 1) * DK] = normed.astype(BF16)
 
     def project(c):
-        resid = resid_v[tile(c), :] + dot(a_v[tile(c), 2 * C : 4 * C], wo_v[2 * C : 4 * C, :])
-        resid_v[tile(c), :] = resid
+        resid_v[tile(c), :] = resid_v[tile(c), :] + dot(
+            a_v[tile(c), 2 * C : 4 * C], wo_v[2 * C : 4 * C, :]
+        )
+
+    def stats(c):
+        resid = resid_v[tile(c), :]
         mean = jnp.sum(resid, axis=1, keepdims=True) * (1.0 / H)
         dev = resid - mean
         m2 = jnp.sum(dev * dev, axis=1, keepdims=True)
@@ -466,17 +523,24 @@
         rec_sends[c].start()
 
     recur_tile(0)
-    pool_project(NT - 1)
-    recur_tile(1)
-    for c in range(NT):
+    pool_sends[0].wait_recv()
+    for k in range(R // B, 3 * R // B):
+        recur(k)
+    pool_project(0)
+    rec_sends[1].start()
+    rec_sends[2].start()
+    rec_sends[0].wait_recv()
+    for k in range(3 * R // B, T // B):
+        recur(k)
+    project(0)
+    rec_sends[3].start()
+    for c in range(1, NT):
         rec_sends[c].wait_recv()
-        if c + 2 < NT:
-            for k in range(R // B):
-                recur((c + 2) * (R // B) + k)
         project(c)
-        if c + 2 < NT:
-            rec_sends[c + 2].start()
-        stat_sends[c].start()
+        stats(c - 1)
+        stat_sends[c - 1].start()
+    stats(NT - 1)
+    stat_sends[NT - 1].start()
     for c in range(NT):
         stat_sends[c].wait_recv()
         norm(c)

time: 35.1 us -> 32.7 us (0.932)
  the two profiles are of different devices: /device:TPU:1 before, /device:TPU:115 now
where the time goes in v4:
time: 32.7 us; the launch traced here: 32.6 us
  Pallas kernels  31.2 us (95%)
  local copies, waits for them, and re-layouts  1.32 us (4%)
    pallas_call x1, Pallas kernels, layer(): pl.pallas_call(functools.partial(kernel, nz), out_shape=pltpu.VMEM((T, H)...  31.2 us
    unnamed x1, local copies, waits for them, and re-layouts  1.32 us

profile of v4, /device:TPU:115, one launch (start us, length us, event | category | flops | bytes accessed | tf_op | source)
XLA Modules:
  0.0 32.6 jit_solution(18309382444403505817)
XLA Ops:
  0.0 31.2 %shard_map.145 = bf16[1024,1024]{1,0:T(8,128)(2,1)S(1)} custom-call(bf16[1024,1024]{1,0:T(8,128)(2,1)} %bitcast.9, bf16[2048,512]{1,0:T(8,128)(2,1)} %wp.1, bf16[2048,512]{1,0:T(8,128)(2,1)} %wq.1, bf16[2048,512]{1,0:T(8,128)(2,1)} %wf.1, bf16[2048,512]{1,0:T(8,128)(2,1)} %wv.1, bf16[2048,512]{1,0:T(8,128)(2,1)} %wg.1, bf16[2,256,256]{2,1,0:T(8,128)(2,1)} %pmix.1, ...), custom_call_target="tpu_custom_call" | custom-call | tf_op jit(solution)/shard_map/pallas_call | solution.py:623
  31.3 1.3 %copy.17 = bf16[1,1024,1024]{2,1,0:T(8,128)(2,1)} copy(bf16[1,1024,1024]{2,1,0:T(8,128)(2,1)S(1)} %bitcast.8) | data formatting | bytes 4194304

commit v5 on v4

--- a/solution.py
+++ b/solution.py
@@ -73,7 +73,7 @@
     out,
     x_v, wf_v, wv_v, wp_v, wq_v, wg_v, wo_v,
     pmix_v, pscale_v, lb_v, ed_v, edc_v, rgain_v, ngain_v, nbias_v,
-    f_v, v_v, explog_v, down_v, pooled_v, halo_v, sq_v, gate_v, a_v,
+    f_v, hl_v, inw_v, end_v, v_v, explog_v, down_v, pooled_v, halo_v, sq_v, gate_v, a_v,
     st_v, cur_v, off_v, offcur_v, band_v, tri_v,
     s1_send, s1_recv, s2_send, s2_recv, s3_send, s3_recv, pre_v, bsum_v, run_v,
     resid_v, stat_v, ostat_v,
@@ -160,9 +160,6 @@
         ).start()
     for c in range(1, NT):
         start_x(c)
-    first[1].start()
-    for k in range(7):
-        params[k].start()
 
     row = lax.broadcasted_iota(jnp.int32, (B, B), 0)
     col = lax.broadcasted_iota(jnp.int32, (B, B), 1)
@@ -180,13 +177,15 @@
     pooled_v[pl.ds(0, B), :] = jnp.zeros((B, C), BF16)
 
     first[0].wait()
+    first[1].start()
+    for k in range(7):
+        params[k].start()
     for c in range(NT):
         loads[c].wait()
         f_v[tile(c), :] = dot(x_v[tile(c), 0:H], wf_v[0:H, :])
 
-    for k in (2, 3):
-        first[k].start()
-    for k in (0, 1, 2, 3):
+    first[2].start()
+    for k in (0, 1, 2):
         second[k].start()
 
     first[1].wait()
@@ -218,13 +217,11 @@
     first[2].wait()
     for c in range(NB_BIG):
         resid_v[big(c), C : 2 * C] = dot(x_v[big(c), 0:H], wp_v[0:H, :])
-    first[4].start()
-    second[4].start()
+    for k in (3, 4):
+        first[k].start()
+        second[k].start()
     for c in out_loads:
         c.start()
-    first[3].wait()
-    for c in range(NB_BIG):
-        gate_v[big(c), :] = dot(x_v[big(c), 0:H], wq_v[0:H, :])
     params[0].wait()
     params[1].wait()
     for b in range(NB):
@@ -232,6 +229,8 @@
 
     def forget_dots(c):
         f_v[tile(c), :] = f_v[tile(c), :] + dot(x_v[tile(c), H : 2 * H], wf_v[H : 2 * H, :])
+
+    def value_dots(c):
         v_v[tile(c), :] = (
             resid_v[tile(c), 0:C] + dot(x_v[tile(c), H : 2 * H], wv_v[H : 2 * H, :])
         ).astype(BF16)
@@ -241,48 +240,71 @@
             resid_v[big(c), C : 2 * C] + dot(x_v[big(c), H : 2 * H], wp_v[H : 2 * H, :])
         ).astype(BF16)
 
-    def forget_block(b):
+    def forget_gate(b):
         rows = pl.ds(b * B, B)
         ed = edc_v[rows, :]
-        off = offcur_v[...]
-        off_v[b] = off
+        for h in range(NH):
+            cols = slice(h * DK, (h + 1) * DK)
+            half_gap = 0.5 - 0.5 * lb_v[:, cols]
+            w_in = half_gap - half_gap * jnp.tanh(0.5 * f_v[rows, cols])
+            f_v[rows, cols] = w_in
+            keep = jnp.log(1.0 - w_in) * LOG2E + ed[:, h : h + 1]
+            hi = keep.astype(BF16)
+            hl_v[b % 4, 0:B, cols] = hi
+            hl_v[b % 4, B : 2 * B, cols] = (keep - hi.astype(F32)).astype(BF16)
+
+    def forget_sums(b):
+        return [dot(tri_v[...], hl_v[b % 4, :, 2 * p * DK : 2 * (p + 1) * DK]) for p in range(NH // 2)]
+
+    def forget_exps(b, sums):
+        rows = pl.ds(b * B, B)
+        off_v[b] = offcur_v[...]
         for p in range(NH // 2):
             cols = slice(2 * p * DK, 2 * (p + 1) * DK)
-            half_gap = 0.5 - 0.5 * lb_v[:, cols]
-            w_in = half_gap - half_gap * jnp.tanh(0.5 * f_v[rows, cols])
-            keep = jnp.log(1.0 - w_in) * LOG2E
-            keep = jnp.concatenate(
-                [keep[:, k * DK : (k + 1) * DK] + ed[:, 2 * p + k : 2 * p + k + 1] for k in range(2)], axis=1
-            )
-            hi = keep.astype(BF16)
-            lo = (keep - hi.astype(F32)).astype(BF16)
-            total = dot(tri_v[...], jnp.concatenate([hi, lo], axis=0))
+            total = sums[p]
             end = total[B - 1 : B, :]
+            w_in = f_v[rows, cols]
             explog_v[rows, cols] = jnp.exp2(total)
             down_v[rows, cols] = (w_in * jnp.exp2(-total)).astype(BF16)
-            inw = (w_in * jnp.exp2(end - total)).astype(BF16)
-            kept = jnp.exp2(end)
-            offcur_v[:, cols] = off[:, cols] + end
-            for k in range(2):
-                h = 2 * p + k
-                hs = slice(k * DK, (k + 1) * DK)
-                st = cur_v[h]
-                st_v[b, h] = st
-                cur_v[h] = kept[:, hs] * st + dot_tn(v_v[rows, h * DK : (h + 1) * DK], inw[:, hs])
+            inw_v[rows, cols] = (w_in * jnp.exp2(end - total)).astype(BF16)
+            end_v[b, :, cols] = end
+            offcur_v[:, cols] = offcur_v[:, cols] + end
+
+    def state_terms(b):
+        rows = pl.ds(b * B, B)
+        kept = jnp.exp2(end_v[b])
+        for h in range(NH):
+            hs = slice(h * DK, (h + 1) * DK)
+            st = cur_v[h]
+            st_v[b, h] = st
+            cur_v[h] = kept[:, hs] * st + dot_tn(v_v[rows, hs], inw_v[rows, hs])
 
     second[0].wait()
     second[1].wait()
+    second[2].wait()
     x_sends[0].wait_recv()
     forget_dots(0)
-    second[2].wait()
+    value_dots(0)
+    for k in range(R // B):
+        forget_gate(k)
     for c in range(NT):
+        blocks = range(c * R // B, (c + 1) * R // B)
         if c + 1 < NT:
             x_sends[c + 1].wait_recv()
+        sums = [forget_sums(b) for b in blocks]
+        if c + 1 < NT:
             forget_dots(c + 1)
         else:
             pooled_dots(0)
-        for s in range(R // B):
-            forget_block(c * (R // B) + s)
+        for b, part in zip(blocks, sums):
+            forget_exps(b, part)
+        if c + 1 < NT:
+            value_dots(c + 1)
+        for b in blocks:
+            state_terms(b)
+        if c + 1 < NT:
+            for b in blocks:
+                forget_gate(b + R // B)
 
     for h in range(NH):
         s1_send[h, pl.ds(0, DK), :] = cur_v[h].astype(BF16)
@@ -309,10 +331,11 @@
     def _():
         halo.start()
 
+    first[3].wait()
     second[3].wait()
 
     def query_dots(c):
-        q = gate_v[tile(c), :] + dot(x_v[tile(c), H : 2 * H], wq_v[H : 2 * H, :])
+        q = dot(x_v[tile(c), :], wq_v[...])
         up = (silu(q) * explog_v[tile(c), :]).astype(BF16)
         for s in range(R // B):
             rows = pl.ds(c * R + s * B, B)
@@ -375,13 +398,21 @@
         for d in (2, 1, 3):
             msg3(d).start()
 
-    @pl.when(x > 0)
-    def _():
-        row_prefix()
-
-        @pl.when(z == 0)
+    row_at = jnp.where(x == 0, 1, 0)
+    column_at = row_at + jnp.where(z == 0, 0, jnp.where(tp == 0, 2, 1))
+
+    def prefixes(at):
+        if at <= 1:
+
+            @pl.when(row_at == at)
+            def _():
+                row_prefix()
+
+        @pl.when(column_at == at)
         def _():
             column_prefix()
+
+    prefixes(0)
 
     first[4].wait()
     second[4].wait()
@@ -421,25 +452,13 @@
     pool_tiles(1)
     pool_sends[1].start()
 
-    @pl.when(x == 0)
-    def _():
-        row_prefix()
-
-        @pl.when(z == 0)
-        def _():
-            column_prefix()
-
-    @pl.when((x > 0) & (z > 0))
-    def _():
-        column_prefix()
+    prefixes(1)
 
     gate_dots(2)
     pool_tiles(2)
     pool_sends[2].start()
 
-    @pl.when((x == 0) & (z > 0))
-    def _():
-        column_prefix()
+    prefixes(2)
 
     @pl.when(jnp.logical_not(is_first))
     def _():
@@ -451,6 +470,7 @@
     pool_tiles(0)
     pool_sends[3].start()
     pool_sends[0].start()
+    prefixes(3)
 
     for c in out_loads:
         c.wait()
@@ -583,6 +603,9 @@
         pltpu.VMEM((1, H), F32),
         pltpu.VMEM((1, H), F32),
         pltpu.VMEM((T, C), F32),
+        pltpu.VMEM((4, 2 * B, C), BF16),
+        pltpu.VMEM((T, C), BF16),
+        pltpu.VMEM((NB, 1, C), F32),
         pltpu.VMEM((T, C), BF16),
         pltpu.VMEM((T, C), F32),
         pltpu.VMEM((T, C), BF16),

time: 32.7 us -> 32.3 us (0.988)
  the two profiles are of different devices: /device:TPU:115 before, /device:TPU:81 now
where the time goes in v5:
time: 32.3 us; the launch traced here: 32.2 us
  Pallas kernels  30.9 us (96%)
  local copies, waits for them, and re-layouts  1.32 us (4%)
    pallas_call x1, Pallas kernels, layer(): pl.pallas_call(functools.partial(kernel, nz), out_shape=pltpu.VMEM((T, H)...  30.9 us
    unnamed x1, local copies, waits for them, and re-layouts  1.32 us

profile of v5, /device:TPU:81, one launch (start us, length us, event | category | flops | bytes accessed | tf_op | source)
XLA Modules:
  0.0 32.2 jit_solution(15782576066560738233)
XLA Ops:
  0.0 30.9 %shard_map.145 = bf16[1024,1024]{1,0:T(8,128)(2,1)S(1)} custom-call(bf16[1024,1024]{1,0:T(8,128)(2,1)} %bitcast.9, bf16[2048,512]{1,0:T(8,128)(2,1)} %wp.1, bf16[2048,512]{1,0:T(8,128)(2,1)} %wq.1, bf16[2048,512]{1,0:T(8,128)(2,1)} %wf.1, bf16[2048,512]{1,0:T(8,128)(2,1)} %wv.1, bf16[2048,512]{1,0:T(8,128)(2,1)} %wg.1, bf16[2,256,256]{2,1,0:T(8,128)(2,1)} %pmix.1, ...), custom_call_target="tpu_custom_call" | custom-call | tf_op jit(solution)/shard_map/pallas_call | solution.py:646
  30.9 1.3 %copy.17 = bf16[1,1024,1024]{2,1,0:T(8,128)(2,1)} copy(bf16[1,1024,1024]{2,1,0:T(8,128)(2,1)S(1)} %bitcast.8) | data formatting | bytes 4194304

commit v6 on v5

--- a/solution.py
+++ b/solution.py
@@ -184,15 +184,6 @@
         loads[c].wait()
         f_v[tile(c), :] = dot(x_v[tile(c), 0:H], wf_v[0:H, :])
 
-    first[2].start()
-    for k in (0, 1, 2):
-        second[k].start()
-
-    first[1].wait()
-    for c in range(NB_BIG):
-        resid_v[big(c), 0:C] = dot(x_v[big(c), 0:H], wv_v[0:H, :])
-    pl.semaphore_wait(barrier, len(greeted) + jnp.minimum(sp, 1) + jnp.minimum(n_sp - 1 - sp, 1))
-
     def send(src, dst, s_sem, r_sem, dev):
         return pltpu.make_async_remote_copy(
             src_ref=src, dst_ref=dst, send_sem=s_sem, recv_sem=r_sem, device_id=dev, device_id_type=MESH
@@ -205,8 +196,26 @@
         )
         for c in range(NT)
     ]
-    for c in x_sends:
-        c.start()
+    def meet_and_send():
+        pl.semaphore_wait(barrier, len(greeted) + jnp.minimum(sp, 1) + jnp.minimum(n_sp - 1 - sp, 1))
+        for c in x_sends:
+            c.start()
+
+    @pl.when(z > 0)
+    def _():
+        meet_and_send()
+
+    first[2].start()
+    for k in (0, 1, 2):
+        second[k].start()
+
+    first[1].wait()
+    for c in range(NB_BIG):
+        resid_v[big(c), 0:C] = dot(x_v[big(c), 0:H], wv_v[0:H, :])
+    @pl.when(z == 0)
+    def _():
+        meet_and_send()
+
     w_sends = [
         send(
             src.at[:, oth_half], wo_v.at[pl.ds((2 * k + 1) * C, C), :], ws_sem.at[k], wr_sem.at[k], partner
@@ -215,8 +224,12 @@
     ]
 
     first[2].wait()
-    for c in range(NB_BIG):
-        resid_v[big(c), C : 2 * C] = dot(x_v[big(c), 0:H], wp_v[0:H, :])
+    resid_v[big(0), C : 2 * C] = dot(x_v[big(0), 0:H], wp_v[0:H, :])
+
+    @pl.when(z == 0)
+    def _():
+        resid_v[big(1), C : 2 * C] = dot(x_v[big(1), 0:H], wp_v[0:H, :])
+
     for k in (3, 4):
         first[k].start()
         second[k].start()
@@ -235,10 +248,13 @@
             resid_v[tile(c), 0:C] + dot(x_v[tile(c), H : 2 * H], wv_v[H : 2 * H, :])
         ).astype(BF16)
 
-    def pooled_dots(c):
+    def pooled_rest(c):
         pooled_v[pl.ds(c * RB + B, RB), :] = (
             resid_v[big(c), C : 2 * C] + dot(x_v[big(c), H : 2 * H], wp_v[H : 2 * H, :])
         ).astype(BF16)
+
+    def pooled_whole(c):
+        pooled_v[pl.ds(c * RB + B, RB), :] = dot(x_v[big(c), :], wp_v[...]).astype(BF16)
 
     def forget_gate(b):
         rows = pl.ds(b * B, B)
@@ -294,8 +310,6 @@
         sums = [forget_sums(b) for b in blocks]
         if c + 1 < NT:
             forget_dots(c + 1)
-        else:
-            pooled_dots(0)
         for b, part in zip(blocks, sums):
             forget_exps(b, part)
         if c + 1 < NT:
@@ -323,7 +337,16 @@
     for c in w_sends:
         c.start()
 
-    pooled_dots(1)
+    pooled_rest(0)
+
+    @pl.when(z == 0)
+    def _():
+        pooled_rest(1)
+
+    @pl.when(z > 0)
+    def _():
+        pooled_whole(1)
+
 
     halo = send(pooled_v.at[pl.ds(T + B - 16, 16), :], halo_v, hs_sem, hr_sem, next_dev)
 
@@ -345,9 +368,6 @@
                 sc = dot_nt(u, down_v[rows, hs])
                 sq_v[rows, 2 * h * DK : (2 * h + 1) * DK] = jnp.where(lower, sc, 0.0).astype(BF16)
                 sq_v[rows, (2 * h + 1) * DK : (2 * h + 2) * DK] = u
-
-    for c in range(NT):
-        query_dots(c)
 
     def msg2(k):
         return send(s2_send, s2_recv.at[z], m2s_sem.at[k], m2r_sem.at[z], {"sp_0": k})
@@ -399,7 +419,7 @@
             msg3(d).start()
 
     row_at = jnp.where(x == 0, 1, 0)
-    column_at = row_at + jnp.where(z == 0, 0, jnp.where(tp == 0, 2, 1))
+    column_at = jnp.where(z == 0, row_at, 2 + row_at)
 
     def prefixes(at):
         if at <= 1:
@@ -412,7 +432,11 @@
         def _():
             column_prefix()
 
+    for c in range(NT - 1):
+        query_dots(c)
     prefixes(0)
+    query_dots(NT - 1)
+    prefixes(1)
 
     first[4].wait()
     second[4].wait()
@@ -452,25 +476,23 @@
     pool_tiles(1)
     pool_sends[1].start()
 
-    prefixes(1)
+    prefixes(2)
 
     gate_dots(2)
+    gate_dots(3)
     pool_tiles(2)
     pool_sends[2].start()
-
-    prefixes(2)
+    prefixes(3)
 
     @pl.when(jnp.logical_not(is_first))
     def _():
         halo.wait_recv()
         pooled_v[pl.ds(B - 16, 16), :] = halo_v[...]
 
-    gate_dots(3)
     pool_tiles(3)
     pool_tiles(0)
     pool_sends[3].start()
     pool_sends[0].start()
-    prefixes(3)
 
     for c in out_loads:
         c.wait()
@@ -561,9 +583,11 @@
         stat_sends[c - 1].start()
     stats(NT - 1)
     stat_sends[NT - 1].start()
-    for c in range(NT):
-        stat_sends[c].wait_recv()
-        norm(c)
+    for group in ((0, 1), (2,), (3,)):
+        for c in group:
+            stat_sends[c].wait_recv()
+        for c in group:
+            norm(c)
 
     for c in range(NT):
         x_sends[c].wait_send()

time: 32.3 us -> 32.9 us (1.019)
  the two profiles are of different devices: /device:TPU:81 before, /device:TPU:1 now
where the time goes in v6:
time: 32.9 us; the launch traced here: 32.8 us
  Pallas kernels  31.5 us (96%)
  local copies, waits for them, and re-layouts  1.32 us (4%)
    pallas_call x1, Pallas kernels, layer(): pl.pallas_call(functools.partial(kernel, nz), out_shape=pltpu.VMEM((T, H)...  31.5 us
    unnamed x1, local copies, waits for them, and re-layouts  1.32 us

profile of v6, /device:TPU:1, one launch (start us, length us, event | category | flops | bytes accessed | tf_op | source)
XLA Modules:
  0.0 32.8 jit_solution(3522244960136026795)
XLA Ops:
  0.0 31.5 %shard_map.145 = bf16[1024,1024]{1,0:T(8,128)(2,1)S(1)} custom-call(bf16[1024,1024]{1,0:T(8,128)(2,1)} %bitcast.9, bf16[2048,512]{1,0:T(8,128)(2,1)} %wp.1, bf16[2048,512]{1,0:T(8,128)(2,1)} %wq.1, bf16[2048,512]{1,0:T(8,128)(2,1)} %wf.1, bf16[2048,512]{1,0:T(8,128)(2,1)} %wv.1, bf16[2048,512]{1,0:T(8,128)(2,1)} %wg.1, bf16[2,256,256]{2,1,0:T(8,128)(2,1)} %pmix.1, ...), custom_call_target="tpu_custom_call" | custom-call | tf_op jit(solution)/shard_map/pallas_call | solution.py:670
  31.5 1.3 %copy.17 = bf16[1,1024,1024]{2,1,0:T(8,128)(2,1)} copy(bf16[1,1024,1024]{2,1,0:T(8,128)(2,1)S(1)} %bitcast.8) | data formatting | bytes 4194304

commit v7 on v5

--- a/solution.py
+++ b/solution.py
@@ -399,7 +399,7 @@
             msg3(d).start()
 
     row_at = jnp.where(x == 0, 1, 0)
-    column_at = row_at + jnp.where(z == 0, 0, jnp.where(tp == 0, 2, 1))
+    column_at = row_at + jnp.where(z == 0, 0, jnp.where((tp == 0) | (z == 2), 2, 1))
 
     def prefixes(at):
         if at <= 1:

time: 32.3 us -> 32.5 us (level)
  no operation moved by 1% of the time
where the time goes in v7:
time: 32.5 us; the launch traced here: 32.3 us
  Pallas kernels  31 us (95%)
  local copies, waits for them, and re-layouts  1.32 us (4%)
    pallas_call x1, Pallas kernels, layer(): pl.pallas_call(functools.partial(kernel, nz), out_shape=pltpu.VMEM((T, H)...  31 us
    unnamed x1, local copies, waits for them, and re-layouts  1.32 us

profile of v7, /device:TPU:81, one launch (start us, length us, event | category | flops | bytes accessed | tf_op | source)
XLA Modules:
  0.0 32.3 jit_solution(17866166354071276578)
XLA Ops:
  0.0 31.0 %shard_map.145 = bf16[1024,1024]{1,0:T(8,128)(2,1)S(1)} custom-call(bf16[1024,1024]{1,0:T(8,128)(2,1)} %bitcast.9, bf16[2048,512]{1,0:T(8,128)(2,1)} %wp.1, bf16[2048,512]{1,0:T(8,128)(2,1)} %wq.1, bf16[2048,512]{1,0:T(8,128)(2,1)} %wf.1, bf16[2048,512]{1,0:T(8,128)(2,1)} %wv.1, bf16[2048,512]{1,0:T(8,128)(2,1)} %wg.1, bf16[2,256,256]{2,1,0:T(8,128)(2,1)} %pmix.1, ...), custom_call_target="tpu_custom_call" | custom-call | tf_op jit(solution)/shard_map/pallas_call | solution.py:646
  31.0 1.3 %copy.17 = bf16[1,1024,1024]{2,1,0:T(8,128)(2,1)} copy(bf16[1,1024,1024]{2,1,0:T(8,128)(2,1)S(1)} %bitcast.8) | data formatting | bytes 4194304
